TPU v7x, 256 devices: a whole 4x4x8 slice. The times are simulated.
256 devices in a mesh: sp: 16 (over y, x), tp: 16 (over z, core).
Axes of the slice: x: 4, y: 4, z: 8, core: 2. Of those that a mesh axis runs over, the one named last changes fastest.
Arguments:
- residual: bfloat16 [6144, 2048], P(('sp', 'tp')), may hold values from -40 to 40
- queries: bfloat16 [6144, 16, 256], P('sp', 'tp'), may hold values from -8.8 to 8.8
- query_rope: bfloat16 [6144, 16, 64], P('sp', 'tp'), may hold values from -72 to 72
- latent: bfloat16 [6144, 512], P('sp'), may hold values from -320 to 320
- key_rope: bfloat16 [6144, 32], P('sp'), may hold values from -48 to 48
- latent_gain: float32 [512], replicated, may hold values from 0.1 to 1.9
- key_weight: bfloat16 [512, 16, 256], P(None, 'tp'), may hold values from -0.25 to 0.25
- value_weight: bfloat16 [512, 16, 256], P(None, 'tp'), may hold values from -0.25 to 0.25
- out_weight: bfloat16 [16, 256, 2048], P('tp'), may hold values from -0.09375 to 0.09375
- norm_gain: float32 [2048], replicated, may hold values from 0.1 to 1.9
- routes: int32 [6144, 2], P('sp'), may hold values from 0 to 31, as said below
- group_gate: float32 [6144], P(('sp', 'tp')), may hold values from 0.5 to 1
- expert_share: float32 [6144, 2], P(('sp', 'tp')), may hold values from 0.2 to 1
- gate_weight: bfloat16 [32, 2048, 4096], P('sp', None, 'tp'), may hold values from -0.125 to 0.125
- up_weight: bfloat16 [32, 2048, 4096], P('sp', None, 'tp'), may hold values from -0.125 to 0.125
- down_weight: bfloat16 [32, 4096, 2048], P('sp', 'tp'), may hold values from -0.1875 to 0.1875
Outputs:
- layer_out: bfloat16 [6144, 2048], P(('sp', 'tp'))
Inputs may be any that keep to these rules, and one draw needn't show every extreme that they name: `routes`: each token names two different experts of one group; expert e belongs to group e // 8. In each aligned block of 24 tokens no expert is named more than 2 times, and one expert, the same in every block, is named exactly 2 times in every block.
All inputs are finite; a program needn't handle non-finite values.
Results may differ from a plain program's by a relative error of at most 0.025.
Values may be sent and summed in bfloat16 or wider, within the bound.
A program may use at most 64 MiB of HBM per device.

v0:
```python
import jax
import jax.numpy as jnp
from jax import lax
from jax.sharding import Mesh
from jax.sharding import PartitionSpec as P

DK_A = 64
DV_A = 64
SP = ("sp_0", "sp_1")
SP_TP = ("sp_0", "sp_1", "tp")


rope_base = 10000.0
epsilon = 1e-06
floor_score = -1e30


def in_blocks(value, dim, count):
    dims = value.shape
    pieces = value.reshape(*dims[:dim], count, dims[dim] // count, *dims[dim + 1 :])
    return jnp.moveaxis(pieces, dim, 0)


def sum_at_owner(value, axis, dim):
    pieces = in_blocks(value, dim, lax.axis_size(axis))
    arrived = lax.all_to_all(pieces, axis, split_axis=0, concat_axis=0, tiled=True)
    return arrived.astype(jnp.float32).sum(axis=0)


def laid_out(pieces, dim):
    dims = list(pieces.shape[1:])
    dims[dim] *= pieces.shape[0]
    return jnp.moveaxis(pieces, 0, dim).reshape(dims)


def turned_blocks(pieces, axes, sequence):
    inside = pieces.shape[1:]
    out = pieces.reshape(*(lax.axis_size(a) for a in axes), *inside)
    for k in sequence:
        out = lax.all_to_all(out, axes[k], k, k, tiled=True)
    return out.reshape(-1, *inside)


def stepwise_exchange(value, axes, sequence, split_dim, concat_dim):
    pieces = in_blocks(value, split_dim, lax.axis_size(axes))
    return laid_out(turned_blocks(pieces, axes, sequence), concat_dim)


def angle_tables(places, rope_width):
    frequencies = rope_base ** (-jnp.arange(0, rope_width, 2, dtype=jnp.float32) / rope_width)
    angles = places[:, None] * frequencies[None, :]
    return (jnp.cos(angles), jnp.sin(angles))


def rope_turn(values, cosine, sine_table):
    half_size = values.shape[-1] // 2
    first_half = values[..., :half_size]
    second = values[..., half_size:]
    return jnp.concatenate(
        [first_half * cosine - second * sine_table, second * cosine + first_half * sine_table],
        axis=-1,
    )


def rms_scale(values, gain_vector):
    values = values.astype(jnp.float32)
    inverse = lax.rsqrt(jnp.mean(values * values, axis=-1, keepdims=True) + epsilon)
    return values * inverse * gain_vector


def online_step(
    carried, query_nope, query_turned, key_nope, piece_rope, value_part, visible, scale
):
    row_top, weight_sum, accumulated = carried
    scores = jnp.einsum("qhd,khd->hqk", query_nope, key_nope, preferred_element_type=jnp.float32)
    scores = scores + jnp.einsum(
        "qhd,kd->hqk", query_turned, piece_rope, preferred_element_type=jnp.float32
    )
    scores = scores * scale
    masked = jnp.where(visible[None], scores, floor_score)
    new_top = jnp.maximum(row_top, jnp.max(masked, axis=2))
    weights = jnp.where(visible[None], jnp.exp(masked - new_top[:, :, None]), 0.0)
    factor = jnp.exp(row_top - new_top)
    weight_sum = weight_sum * factor + jnp.sum(weights, axis=2)
    update = jnp.einsum(
        "hqk,khd->qhd", weights.astype(jnp.bfloat16), value_part, preferred_element_type=jnp.float32
    )
    accumulated = accumulated * jnp.transpose(factor)[:, :, None] + update
    return (new_top, weight_sum, accumulated)


def slot_table(route_block, experts_all, capacity):
    flat_routes = route_block.reshape(-1)
    onehot = (flat_routes[:, None] == jnp.arange(experts_all, dtype=jnp.int32)[None, :]).astype(
        jnp.int32
    )
    rank_within = jnp.sum((jnp.cumsum(onehot, axis=0) - onehot) * onehot, axis=1)
    return flat_routes * capacity + rank_within


def local(
    residual,
    queries,
    query_rope,
    latent,
    key_rope,
    latent_gain,
    key_weight,
    value_weight,
    out_weight,
    norm_gain,
    routes,
    group_gate,
    expert_share,
    gate_weight,
    up_weight,
    down_weight,
):
    local_tokens = queries.shape[0]
    pair_dev = queries.shape[1]
    sp_count = lax.axis_size(SP)
    tp_count = lax.axis_size("tp")
    row_count = local_tokens // tp_count
    rope_width = key_rope.shape[1]
    first_place = lax.axis_index(SP) * local_tokens
    places = (first_place + jnp.arange(local_tokens, dtype=jnp.int32)).astype(jnp.float32)
    cosine, sine_table = angle_tables(places, rope_width)
    rotated_key = rope_turn(key_rope.astype(jnp.float32), cosine, sine_table).astype(jnp.bfloat16)
    turned = rope_turn(
        query_rope.astype(jnp.float32).reshape(local_tokens, pair_dev, 2, rope_width),
        cosine[:, None, None, :],
        sine_table[:, None, None, :],
    ).astype(jnp.bfloat16)
    compressed = rms_scale(latent, latent_gain).astype(jnp.bfloat16)
    scale_one = (DK_A + rope_width) ** (-0.5)
    scale_two = (queries.shape[2] - DK_A + rope_width) ** (-0.5)
    key_flat = key_weight.reshape(key_weight.shape[0], -1)
    value_flat = value_weight.reshape(value_weight.shape[0], -1)

    def attend_piece(carried, piece_keys, piece_values, piece_rope, piece_start):
        key_count = piece_keys.shape[0]
        key_places = (piece_start + jnp.arange(key_count, dtype=jnp.int32)).astype(jnp.float32)
        visible = places[:, None] >= key_places[None, :]
        state_one = online_step(
            carried[0],
            queries[:, :, :DK_A],
            turned[:, :, 0],
            piece_keys[:, :, :DK_A],
            piece_rope,
            piece_values[:, :, :DV_A],
            visible,
            scale_one,
        )
        state_two = online_step(
            carried[1],
            queries[:, :, DK_A:],
            turned[:, :, 1],
            piece_keys[:, :, DK_A:],
            piece_rope,
            piece_values[:, :, DV_A:],
            visible,
            scale_two,
        )
        return (state_one, state_two)

    def empty_state(value_size):
        return (
            jnp.full((pair_dev, local_tokens), floor_score, jnp.float32),
            jnp.zeros((pair_dev, local_tokens), jnp.float32),
            jnp.zeros((local_tokens, pair_dev, value_size), jnp.float32),
        )

    initial = (empty_state(DV_A), empty_state(value_weight.shape[2] - DV_A))

    def latent_step(carried, sub_pieces, block_start):
        key_count = sub_pieces[0].shape[0]
        piece_keys = (
            jnp.dot(sub_pieces[0], key_flat, preferred_element_type=jnp.float32)
            .astype(jnp.bfloat16)
            .reshape(key_count, pair_dev, -1)
        )
        piece_values = (
            jnp.dot(sub_pieces[0], value_flat, preferred_element_type=jnp.float32)
            .astype(jnp.bfloat16)
            .reshape(key_count, pair_dev, -1)
        )
        return attend_piece(carried, piece_keys, piece_values, sub_pieces[1], block_start)

    carried = initial
    pieces = (
        lax.all_gather(compressed, SP, axis=0, tiled=True),
        lax.all_gather(rotated_key, SP, axis=0, tiled=True),
    )
    key_count = pieces[0].shape[0]
    blocks = key_count // local_tokens
    block_size = key_count // blocks

    def one_block(running, block_index):
        block_start = block_index * block_size
        sub_pieces = tuple(
            (
                lax.dynamic_slice_in_dim(member, block_index * block_size, block_size, 0)
                for member in pieces
            )
        )

        def compute(running_state):
            return latent_step(running_state, sub_pieces, block_start)

        def keep_state(running_state):
            return running_state

        return (
            lax.cond(block_start < first_place + local_tokens, compute, keep_state, running),
            None,
        )

    carried, unused = lax.scan(one_block, carried, jnp.arange(blocks, dtype=jnp.int32))
    part_one = carried[0][2] / jnp.transpose(carried[0][1])[:, :, None]
    part_two = carried[1][2] / jnp.transpose(carried[1][1])[:, :, None]
    attention = (
        jnp.concatenate([part_one, part_two], axis=2).astype(jnp.bfloat16).reshape(local_tokens, -1)
    )
    out_flat = out_weight.reshape(-1, out_weight.shape[2])
    head_total = sum_at_owner(
        jnp.dot(attention, out_flat, preferred_element_type=jnp.float32).astype(jnp.bfloat16),
        "tp",
        0,
    )
    mixed_rows = residual.astype(jnp.float32) + head_total
    normed = rms_scale(mixed_rows, norm_gain).astype(jnp.bfloat16)
    experts_dev = gate_weight.shape[0]
    experts_all = experts_dev * sp_count
    top_count = routes.shape[1]
    capacity = max(2, 3 * row_count * top_count // (2 * experts_all))
    slot_count = experts_all * capacity
    own_routes = lax.dynamic_slice_in_dim(routes, lax.axis_index("tp") * row_count, row_count, 0)
    own_slots = slot_table(own_routes, experts_all, capacity)
    pick_matrix = (jnp.arange(slot_count, dtype=jnp.int32)[:, None] == own_slots[None, :]).astype(
        jnp.bfloat16
    )
    pick_matrix = pick_matrix.reshape(slot_count, row_count, top_count).sum(axis=2)
    outgoing = (
        jnp.dot(pick_matrix, normed, preferred_element_type=jnp.float32)
        .astype(jnp.bfloat16)
        .reshape(sp_count, experts_dev, capacity, -1)
    )
    arrived = stepwise_exchange(outgoing, SP, (0, 1), 0, 0)
    gathered = lax.all_gather(arrived, "tp", axis=0, tiled=True)
    gate_out = jnp.einsum(
        "secd,edf->secf", gathered, gate_weight, preferred_element_type=jnp.float32
    )
    up_out = jnp.einsum("secd,edf->secf", gathered, up_weight, preferred_element_type=jnp.float32)
    hidden = (jax.nn.silu(gate_out) * up_out).astype(jnp.bfloat16)
    expert_out = lax.psum_scatter(
        jnp.einsum(
            "secf,efd->secd", hidden, down_weight, preferred_element_type=jnp.float32
        ).astype(jnp.bfloat16),
        "tp",
        scatter_dimension=0,
        tiled=True,
    )
    returned = lax.all_to_all(expert_out, SP, split_axis=0, concat_axis=0, tiled=True).reshape(
        slot_count, -1
    )
    selectors = (own_slots[:, None] == jnp.arange(slot_count, dtype=jnp.int32)[None, :]).astype(
        jnp.bfloat16
    )
    picked = jnp.dot(selectors, returned, preferred_element_type=jnp.float32).reshape(
        row_count, top_count, -1
    )
    route_weight = group_gate[:, None] * expert_share / jnp.sum(expert_share, axis=1, keepdims=True)
    expert_mix = jnp.sum(route_weight[:, :, None] * picked, axis=1)
    return (mixed_rows + expert_mix).astype(jnp.bfloat16)


def solution(mesh):
    finer = Mesh(mesh.devices.reshape(4, 4, mesh.shape["tp"]), ("sp_0", "sp_1", "tp"))
    placed = (
        P(SP_TP, None),
        P(SP, "tp", None),
        P(SP, "tp", None),
        P(SP, None),
        P(SP, None),
        P(),
        P(None, "tp", None),
        P(None, "tp", None),
        P("tp", None, None),
        P(),
        P(SP, None),
        P(SP_TP),
        P(SP_TP, None),
        P(SP, None, "tp"),
        P(SP, None, "tp"),
        P(SP, "tp", None),
    )
    return jax.shard_map(
        local, mesh=finer, in_specs=placed, out_specs=P(SP_TP, None), check_vma=False
    )
```

profile of v0, /device:TPU:2, one launch (start us, length us, event | category | flops | bytes accessed | tf_op | source)
XLA Modules:
  0.0 414.6 jit_solution(4642356729133802314)
XLA Ops:
  6.5 1.3 fusion.69
  7.9 1.9 fusion.71
  9.8 1.1 copy.39
  11.0 0.7 convert_element_type.111
  11.9 24.3 %all_gather.10 = bf16[6144,32]{0,1:T(8,128)(2,1)S(1)} all-gather(bf16[384,32]{0,1:T(8,128)(2,1)S(1)} %pad_maximum_fusion.1), channel_id=1, replica_groups=mesh['sp_0'=4,'sp_1'=4,'tp'=16] {'sp_0','sp_1'}, dimensions={0}, use_global_device_ids=true | all-gather | bytes 417792 | tf_op jit(solution)/shard_map/all_gather | solution.py:192
  36.2 1.5 copy.40
  37.8 41.7 %all-gather.3.cloned.1.call-done = bf16[6144,512]{1,0:T(8,128)(2,1)} async-done(((bf16[384,512]{1,0:T(8,128)(2,1)}), bf16[6144,512]{1,0:T(8,128)(2,1)}) %all-gather.3.cloned.1.call-update) | async-done | bytes 6291472 | tf_op jit(solution)/shard_map/all_gather | solution.py:191
  79.5 34.3 %while.23 = (s32[]{:T(128)}, f32[1,384]{1,0:T(1,128)S(1)}, f32[1,384]{1,0:T(1,128)S(1)}, f32[384,1,64]{0,2,1:T(8,128)S(1)}, f32[1,384]{1,0:T(1,128)S(1)}, /*inde...) while((s32[]{:T(128)}, f32[1,384]{1,0:T(1,128)S(1)}, ...), condition=%wide.region_8.9_spmd.clone, body=%wide.region_1.8_spmd.clone.sunk | while | flops 375279360 | bytes 9301477 | solution.py:218
  79.6 0.6 dynamic_slice.43
  80.8 6.7 %conditional.3 = ((f32[1,384]{1,0:T(1,128)S(1)}, f32[1,384]{1,0:T(1,128)S(1)}, f32[384,1,64]{0,2,1:T(8,128)S(1)}, f32[1,384]{1,0:T(1,128)S(1)}, f32[1,384]{1,0:T(1,128)S(1)}, /*index=5*/f32[384,1,192]{0,2,1:T(8,128)S(1)})) conditional(s32[]{:T(128)} %convert_element_type.180, (f32[1,384]{1,0:T(1,128)S(1)}, f32[1,384]{1,0:T(1,128)S(1)}, ...), branch_computations={%region_2.2_spmd, %region_3.7_spmd} | conditional | flops 375278592 | bytes 9299566 | solution.py:214
  80.9 1.4 fusion.9
  82.2 0.3 convolution_bitcast_fusion.3
  82.5 1.1 fusion.89
  83.7 1.1 convolution_bitcast_fusion.1
  84.8 0.3 fusion.88
  85.1 0.2 fusion.15
  85.4 1.4 fusion.10
  86.8 0.3 fusion.11
  87.1 0.4 fusion.8
  87.5 0.6 dynamic_slice.43
  88.8 6.7 %conditional.3 = ((f32[1,384]{1,0:T(1,128)S(1)}, f32[1,384]{1,0:T(1,128)S(1)}, f32[384,1,64]{0,2,1:T(8,128)S(1)}, f32[1,384]{1,0:T(1,128)S(1)}, f32[1,384]{1,0:T(1,128)S(1)}, /*index=5*/f32[384,1,192]{0,2,1:T(8,128)S(1)})) conditional(s32[]{:T(128)} %convert_element_type.180, (f32[1,384]{1,0:T(1,128)S(1)}, f32[1,384]{1,0:T(1,128)S(1)}, ...), branch_computations={%region_2.2_spmd, %region_3.7_spmd} | conditional | flops 375278592 | bytes 9299566 | solution.py:214
  88.8 1.4 fusion.9
  90.2 0.3 convolution_bitcast_fusion.3
  90.5 1.1 fusion.89
  91.7 1.1 convolution_bitcast_fusion.1
  92.8 0.3 fusion.88
  93.1 0.2 fusion.15
  93.4 1.4 fusion.10
  94.8 0.3 fusion.11
  95.1 0.4 fusion.8
  95.5 0.6 dynamic_slice.43
  96.8 0.6 dynamic_slice.43
  98.2 0.6 dynamic_slice.43
  99.5 0.6 dynamic_slice.43
  100.8 0.6 dynamic_slice.43
  102.1 0.6 dynamic_slice.43
  103.4 0.6 dynamic_slice.43
  104.7 0.6 dynamic_slice.43
  106.0 0.6 dynamic_slice.43
  107.3 0.6 dynamic_slice.43
  108.7 0.6 dynamic_slice.43
  110.0 0.6 dynamic_slice.43
  111.3 0.6 dynamic_slice.43
  112.6 0.6 dynamic_slice.43
  114.0 3.0 convolution_convert_fusion.2
  117.0 7.3 %all-to-all-start = ((bf16[16,24,2048]{2,1,0:T(8,128)(2,1)}), bf16[16,24,2048]{2,1,0:T(8,128)(2,1)}, u32[]{:S(2)}, u32[]{:S(2)}) async-start(bf16[16,24,2048]{2,1,0:T(8,128)(2,1)} %bitcast.146), calls=%async_computation | async-start | bytes 3145728 | tf_op jit(solution)/shard_map/all_to_all | solution.py:26
  124.3 0.8 constant_dynamic-slice_fusion
  125.9 36.3 %all-to-all-done = bf16[16,24,2048]{2,1,0:T(8,128)(2,1)} async-done(((bf16[16,24,2048]{2,1,0:T(8,128)(2,1)}), bf16[16,24,2048]{2,1,0:T(8,128)(2,1)}, u32[]{:S(2)}, u32[]{:S(2)}) %all-to-all-start) | async-done | bytes 1572896 | tf_op jit(solution)/shard_map/all_to_all | solution.py:26
  162.2 1.7 convert_reduce_fusion
  164.0 0.3 convolution_convert_fusion.3
  164.5 90.4 %all_to_all.20 = bf16[4,4,1,2,2,2048]{5,4,3,1,2,0:T(2,128)(2,1)S(1)} all-to-all(bf16[4,4,1,2,2,2048]{5,4,3,1,2,0:T(2,128)(2,1)S(1)} %bitcast.147), channel_id=1, replica_groups=mesh['sp_0'=4,'sp_1'=4,'tp'=16] {'sp_0'}, dimensions={0} | all-to-all | bytes 524288 | tf_op jit(solution)/shard_map/all_to_all | solution.py:40
  255.0 0.2 copy.45
  255.2 22.3 %all_to_all.21 = bf16[4,4,1,2,2,2048]{5,4,3,0,2,1:T(2,128)(2,1)S(1)} all-to-all(bf16[4,4,1,2,2,2048]{5,4,3,0,2,1:T(2,128)(2,1)S(1)} %copy.45), channel_id=1, replica_groups=mesh['sp_0'=4,'sp_1'=4,'tp'=16] {'sp_1'}, dimensions={1} | all-to-all | bytes 524288 | tf_op jit(solution)/shard_map/all_to_all | solution.py:40
  277.5 0.2 copy.46
  277.7 0.8 reshape_reshape.3
  278.5 37.2 %all-gather.5.cloned.1.call-done = bf16[256,2,2,2048]{3,0,2,1:T(8,128)(2,1)} async-done(((bf16[16,2,2,2048]{3,0,2,1:T(8,128)(2,1)}), bf16[256,2,2,2048]{3,0,2,1:T(8,128)(2,1)}) %all-gather.5.cloned.1.call-update) | async-done | bytes 4194320 | tf_op jit(solution)/shard_map/all_gather | solution.py:249
  315.7 5.2 %fusion.53 = f32[256,2,2,256]{3,0,2,1:T(8,128)} fusion(bf16[256,2,2,2048]{3,0,2,1:T(8,128)(2,1)} %all-gather.5.cloned.1.call-done, bf16[2,2048,256]{2,1,0:T(8,128)(2,1)} %param.33), kind=kOutput, calls=%fused_computation.77 | convolution fusion | flops 1073741824 | bytes 7340032 | tf_op jit(solution)/shard_map/secd,edf->secf/dot_general | solution.py:250
  320.9 7.5 %convert_bitcast_fusion = bf16[256,2,2,2048]{3,0,2,1:T(8,128)(2,1)} fusion(bf16[2,256,2048]{2,1,0:T(8,128)(2,1)S(1)} %copy-done, bf16[256,2,2,2048]{3,0,2,1:T(8,128)(2,1)} %all-gather.5.cloned.1.call-done, bf16[2,2048,256]{2,1,0:T(8,128)(2,1)} %param.34, f32[256,2,2,256]{3,0,2,1:T(8,128)} %fusion.53), kind=kOutput, calls=%fused_computation.67 | convolution fusion | flops 2151153664 | bytes 13631488 | tf_op jit(solution)/shard_map/secf,efd->secd/dot_general | solution.py:256
  328.4 62.1 %reduce-scatter.2.cloned.1.call-done = bf16[16,2,2,2048]{3,0,2,1:T(8,128)(2,1)} async-done(((bf16[256,2,2,2048]{3,0,2,1:T(8,128)(2,1)}), bf16[16,2,2,2048]{3,0,2,1:T(8,128)(2,1)}) %reduce-scatter.2.cloned.1.call-update) | async-done | bytes 262160 | tf_op jit(solution)/shard_map/reduce_scatter | solution.py:255
  390.6 1.9 copy.47
  392.5 7.3 %all-to-all-start.3 = ((bf16[16,2,2,2048]{3,2,1,0:T(2,128)(2,1)}), bf16[16,2,2,2048]{3,2,1,0:T(2,128)(2,1)S(1)}, u32[]{:S(2)}, u32[]{:S(2)}) async-start(bf16[16,2,2,2048]{3,2,1,0:T(2,128)(2,1)} %copy.47), calls=%async_computation.4 | async-start | bytes 524288 | tf_op jit(solution)/shard_map/all_to_all | solution.py:263
  399.8 7.3 %all-to-all-done.3 = bf16[16,2,2,2048]{3,2,1,0:T(2,128)(2,1)S(1)} async-done(((bf16[16,2,2,2048]{3,2,1,0:T(2,128)(2,1)}), bf16[16,2,2,2048]{3,2,1,0:T(2,128)(2,1)S(1)}, u32[]{:S(2)}, u32[]{:S(2)}) %all-to-all-start.3) | async-done | bytes 262176 | tf_op jit(solution)/shard_map/all_to_all | solution.py:263
  407.2 0.3 fusion.65
  407.4 0.7 add_convert_fusion.2
  (98 shorter events, 2.2 us)
Async XLA Ops:
  6.5 314.4 %copy-start = (bf16[2,256,2048]{2,1,0:T(8,128)(2,1)S(1)}, bf16[2,256,2048]{2,1,0:T(8,128)(2,1)}, u32[]{:S(2)}) copy-start(bf16[2,256,2048]{2,1,0:T(8,128)(2,1)} %param.35) | copy-start | bytes 6291460
  6.5 72.9 %all-gather.3.cloned.1.call-start = ((), (), s32[]{:S(2)}) async-start(), calls=%async_computation.5 | async-start | bytes 6684672 | tf_op jit(solution)/shard_map/all_gather | solution.py:191
  7.9 29.9 %copy-start.4 = (bf16[384,1,64]{0,2,1:T(8,128)(2,1)S(1)}, bf16[384,1,64]{0,2,1:T(8,128)(2,1)}, u32[]{:S(2)}) copy-start(bf16[384,1,64]{0,2,1:T(8,128)(2,1)} %param.22) | copy-start | bytes 147460
  9.8 69.8 %copy-start.1 = (bf16[512,1,256]{2,0,1:T(8,128)(2,1)S(1)}, bf16[512,1,256]{2,0,1:T(8,128)(2,1)}, u32[]{:S(2)}) copy-start(bf16[512,1,256]{2,0,1:T(8,128)(2,1)} %param.26) | copy-start | bytes 786436
  9.8 69.8 %copy-start.2 = (bf16[512,1,256]{2,0,1:T(8,128)(2,1)S(1)}, bf16[512,1,256]{2,0,1:T(8,128)(2,1)}, u32[]{:S(2)}) copy-start(bf16[512,1,256]{2,0,1:T(8,128)(2,1)} %param.27) | copy-start | bytes 786436
  117.0 46.9 %copy-start.3 = (bf16[24,2048]{1,0:T(8,128)(2,1)S(1)}, bf16[24,2048]{1,0:T(8,128)(2,1)}, u32[]{:S(2)}) copy-start(bf16[24,2048]{1,0:T(8,128)(2,1)} %param.20) | copy-start | bytes 294916
  117.0 47.1 %copy-start.5 = (f32[2048]{0:T(1024)S(1)}, f32[2048]{0:T(1024)}, u32[]{:S(2)}) copy-start(f32[2048]{0:T(1024)} %param.29) | copy-start | bytes 24580
  117.0 45.2 %all-to-all-start = ((bf16[16,24,2048]{2,1,0:T(8,128)(2,1)}), bf16[16,24,2048]{2,1,0:T(8,128)(2,1)}, u32[]{:S(2)}, u32[]{:S(2)}) async-start(bf16[16,24,2048]{2,1,0:T(8,128)(2,1)} %bitcast.146), calls=%async_computation | async-start | bytes 3145728 | tf_op jit(solution)/shard_map/all_to_all | solution.py:26
  124.3 191.4 %all-gather.5.cloned.1.call-start = ((), (), s32[]{:S(2)}) async-start(), calls=%async_computation.6 | async-start | bytes 4456448 | tf_op jit(solution)/shard_map/all_gather | solution.py:249
  278.5 112.1 %reduce-scatter.2.cloned.1.call-start = ((), (), s32[]{:S(2)}) async-start(), calls=%async_computation.7 | async-start | bytes 4456448 | tf_op jit(solution)/shard_map/reduce_scatter | solution.py:255
  328.4 71.4 %copy-start.6 = (f32[24,2]{0,1:T(2,128)S(1)}, f32[24,2]{0,1:T(2,128)}, u32[]{:S(2)}) copy-start(f32[24,2]{0,1:T(2,128)} %param.32) | copy-start | bytes 580
  328.4 71.4 %copy-start.7 = (f32[24]{0:T(128)S(1)}, f32[24]{0:T(128)}, u32[]{:S(2)}) copy-start(f32[24]{0:T(128)} %param.31) | copy-start | bytes 292
  392.5 14.6 %all-to-all-start.3 = ((bf16[16,2,2,2048]{3,2,1,0:T(2,128)(2,1)}), bf16[16,2,2,2048]{3,2,1,0:T(2,128)(2,1)S(1)}, u32[]{:S(2)}, u32[]{:S(2)}) async-start(bf16[16,2,2,2048]{3,2,1,0:T(2,128)(2,1)} %copy.47), calls=%async_computation.4 | async-start | bytes 524288 | tf_op jit(solution)/shard_map/all_to_all | solution.py:263
Sparse Core Ops, SparseCore 0:
  9.9 69.4 all-gather.2
  278.6 37.0 all-gather.4
  328.5 61.9 reduce-scatter.1
where the time goes:
time: 418 us; the launch traced here: 415 us
  waiting for transfers between devices  185 us (44%)
  blocking collectives  137 us (33%)
  matrix products  28.7 us (7%)
  local copies, waits for them, and re-layouts  16.9 us (4%)
  starting transfers between devices  14.7 us (4%)
  between operations  13.3 us (3%)
  loops' own time  11.4 us (3%)
  other arithmetic  7.94 us (2%)
    all_to_all x2, blocking collectives, turned_blocks(): out = lax.all_to_all(out, axes[k], k, k, tiled=True)  113 us
    reduce_scatter x1, waiting for transfers between devices, local(): lax.psum_scatter(jnp.einsum('secf,efd->secd', hidden, down_weight, prefer...  62.1 us
    all_gather x1, waiting for transfers between devices, local(): lax.all_gather(compressed, SP, axis=0, tiled=True)  41.7 us
    all_gather x1, waiting for transfers between devices, local(): gathered = lax.all_gather(arrived, 'tp', axis=0, tiled=True)  37.2 us
    all_to_all x1, waiting for transfers between devices, sum_at_owner(): lax.all_to_all(pieces, axis, split_axis=0, concat_axis=0, tiled=True)  36.3 us
    all_gather x1, blocking collectives, local(): lax.all_gather(rotated_key, SP, axis=0, tiled=True)  24.3 us
    another operation x1, loops' own time, local(): lax.scan(one_block, carried, jnp.arange(blocks, dtype=jnp.int32))  10.9 us
    dynamic_slice x16, local copies, waits for them, and re-layouts, local(): lax.scan(one_block, carried, jnp.arange(blocks, dtype=jnp.int32))  9.73 us
  transfers between devices with their start and end apart: 5, of which 5 were waited for; matrix products, arithmetic and copies ran while one was open for 1% of the time, Pallas kernels for 0%

commit v1 on v0

v1 whole, which is shorter than its diff:
```python
import functools

import jax
import jax.numpy as jnp
from jax import lax
from jax.experimental import pallas as pl
from jax.experimental.pallas import tpu as pltpu
from jax.sharding import Mesh
from jax.sharding import PartitionSpec as P

DK_A = 64
DV_A = 64
SP = ("y", "x")
TP = ("z", "c")
SP_TP = ("y", "x", "z", "c")
MESH = pl.DeviceIdType.MESH
LOG2E = 1.4426950408889634
BF = jnp.bfloat16
F32 = jnp.float32

rope_base = 10000.0
epsilon = 1e-06
floor_score = -1e30

ORDER = (
    (0, 0),
    (0, 1), (0, 3), (1, 0), (3, 0),
    (0, 2), (2, 0),
    (1, 1), (1, 3), (3, 1), (3, 3),
    (1, 2), (3, 2), (2, 1), (2, 3),
    (2, 2),
)
SLOT = {place: k for k, place in enumerate(ORDER)}
HALF = 208
PART = 112


def place():
    return tuple(lax.axis_index(name) for name in ("y", "x", "z", "c"))


def meet(devices):
    barrier = pltpu.get_barrier_semaphore()
    for device in devices:
        pl.semaphore_signal(barrier, inc=1, device_id=device, device_id_type=MESH)
    pl.semaphore_wait(barrier, len(devices))


def attend_kernel(
    q_ref, own_ref, wk_ref, wv_ref, ow_ref, out_ref,
    buf, kta, ktb, vx, acc, top, owp, attx, attr, part,
    far_out, far_in, step_out, step_in,
    ring_send, ring_recv, flip_send, flip_recv, misc_send, misc_recv, z_send, z_recv,
    *, scale_one, scale_two,
):
    y, x, z, c = place()
    partner = (y, x, z, 1 - c)

    def along_a(step):
        return ((y + c * step + 4) % 4, (x + (1 - c) * step + 4) % 4, z, c)

    def along_b(step):
        return ((y + (1 - c) * step + 4) % 4, (x + c * step + 4) % 4, z, c)

    def along_z(step):
        return (y, x, (z + step + 8) % 8, c)

    def slot(da, db):
        first = SLOT[(db % 4, da % 4)]
        second = SLOT[(da % 4, db % 4)]
        return first if first == second else first + c * (second - first)

    meet(
        [partner, along_a(1), along_a(-1), along_b(1), along_b(-1), along_z(1), along_z(-1)]
    )
    start_row = c * HALF
    other_row = (1 - c) * HALF
    counts = {"ring": 0}
    ring = []

    def piece(k, first, size):
        return buf.at[k - 1, pl.ds(pl.multiple_of(start_row + first, 16), size)]

    spans = {None: (0, HALF), 0: (0, PART), 1: (PART, HALF - PART)}

    def send(source, target, device, which=None):
        first, size = spans[which]
        if source is None:
            src = own_ref.at[pl.ds(pl.multiple_of(start_row + first, 16), size)]
        else:
            src = piece(source, first, size)
        copy = pltpu.make_async_remote_copy(
            src_ref=src,
            dst_ref=piece(target, first, size),
            send_sem=ring_send.at[counts["ring"]],
            recv_sem=ring_recv.at[target - 1, which or 0],
            device_id=device,
            device_id_type=MESH,
        )
        ring.append((counts["ring"], size))
        counts["ring"] += 1
        copy.start()

    def arrived(k, which=None):
        first, size = spans[which]
        pltpu.make_async_remote_copy(
            src_ref=piece(k, first, size),
            dst_ref=piece(k, first, size),
            send_sem=ring_send.at[0],
            recv_sem=ring_recv.at[k - 1, which or 0],
            device_id=partner,
            device_id_type=MESH,
        ).wait_recv()

    def flip(k):
        copy = pltpu.make_async_remote_copy(
            src_ref=piece(k, 0, HALF),
            dst_ref=piece(k, 0, HALF),
            send_sem=flip_send.at[k - 1],
            recv_sem=flip_recv.at[k - 1],
            device_id=partner,
            device_id_type=MESH,
        )
        copy.start()

    def flipped(k):
        there = buf.at[k - 1, pl.ds(pl.multiple_of(other_row, 16), HALF)]
        pltpu.make_async_remote_copy(
            src_ref=there, dst_ref=there,
            send_sem=flip_send.at[0], recv_sem=flip_recv.at[k - 1],
            device_id=partner, device_id_type=MESH,
        ).wait_recv()

    for sign in (1, -1):
        send(None, slot(-sign, 0), along_a(sign))
        send(None, slot(0, -sign), along_b(sign))
    weights_over = pltpu.make_async_remote_copy(
        src_ref=ow_ref, dst_ref=owp, send_sem=misc_send.at[0], recv_sem=misc_recv.at[0],
        device_id=partner, device_id_type=MESH,
    )
    weights_over.start()

    kta[96:128] = jnp.zeros((32, 384), BF)
    ktb[224:256] = jnp.zeros((32, 384), BF)
    lanes = lax.broadcasted_iota(jnp.int32, (1, 384), 1)
    ones = jnp.where((lanes == 64) | (lanes == 320), 1.0, 0.0)
    heads = (
        (slice(0, 128), kta, 0, scale_one * LOG2E),
        (slice(128, 384), ktb, 1, scale_two * LOG2E),
    )

    def block(ref, first):
        rope = ref[0:32, 0:384]
        lat = ref[32:416, :]
        keys = lax.dot_general(
            wk_ref[...], lat, (((1,), (1,)), ((), ())), preferred_element_type=F32
        ).astype(BF)
        kta[0:64] = keys[0:64]
        kta[64:96] = rope
        ktb[0:192] = keys[64:256]
        ktb[192:224] = rope
        vx[...] = (jnp.dot(lat, wv_ref[...], preferred_element_type=F32) + ones).astype(BF)
        for cols, keys_ref, h, factor in heads:
            scores = jnp.dot(q_ref[:, cols], keys_ref[...], preferred_element_type=F32)
            if first:
                rows = lax.broadcasted_iota(jnp.int32, (384, 384), 0)
                places = lax.broadcasted_iota(jnp.int32, (384, 384), 1)
                scores = jnp.where(rows >= places, scores, floor_score)
            peak = jnp.max(scores, axis=1, keepdims=True)
            width = (cols.stop - cols.start) // 128
            if first:
                new = jnp.broadcast_to(peak, (384, 128))
            else:
                old = top[h]
                new = jnp.maximum(old, peak)
            top[h] = new
            weights = jnp.exp2(
                (scores - jnp.concatenate([new] * 3, axis=1)) * factor
            ).astype(BF)
            update = jnp.dot(weights, vx[:, cols], preferred_element_type=F32)
            if first:
                acc[:, cols] = update
            else:
                shrink = jnp.exp2((old - new) * factor)
                acc[:, cols] = acc[:, cols] * jnp.concatenate([shrink] * width, axis=1) + update

    block(own_ref, True)

    me = y * 4 + x

    def step(i, carry):
        @pl.when(i == 1)
        def _():
            near = []
            for sign in (1, -1):
                k = slot(-sign, 0)
                arrived(k)
                flip(k)
                send(k, slot(-2 * sign, 0), along_a(sign), 0 if sign == 1 else 1)
                near.append(k)
                k = slot(0, -sign)
                arrived(k)
                flip(k)
                send(k, slot(0, -2 * sign), along_b(sign), 0 if sign == 1 else 1)
            for sign, k in zip((1, -1), near):
                send(k, slot(-sign, -1), along_b(1))
                send(k, slot(-sign, 1), along_b(-1))

        @pl.when(i == 5)
        def _():
            k = slot(2, 0)
            arrived(k, 0)
            arrived(k, 1)
            flip(k)
            send(k, slot(2, -1), along_b(1))
            send(k, slot(2, 1), along_b(-1))
            k = slot(0, 2)
            arrived(k, 0)
            arrived(k, 1)
            flip(k)

        @pl.when(i == 7)
        def _():
            for da in (-1, 1):
                for sign in (1, -1):
                    k = slot(da, -sign)
                    arrived(k)
                    flip(k)
                    send(k, slot(da, -2 * sign), along_b(sign), 0 if sign == 1 else 1)

        @pl.when(i == 11)
        def _():
            for sign in (1, -1):
                k = slot(2, -sign)
                arrived(k)
                flip(k)
                send(k, slot(2, -2 * sign), along_b(sign), 0 if sign == 1 else 1)
            for da in (-1, 1):
                k = slot(da, 2)
                arrived(k, 0)
                arrived(k, 1)
                flip(k)

        @pl.when(i == 15)
        def _():
            k = slot(2, 2)
            arrived(k, 0)
            arrived(k, 1)
            flip(k)

        flipped(i)
        dy = 0
        dx = 0
        for k in range(1, 16):
            dy = jnp.where(i == k, ORDER[k][0], dy)
            dx = jnp.where(i == k, ORDER[k][1], dx)
        theirs = ((y + dy) % 4) * 4 + (x + dx) % 4

        @pl.when(theirs < me)
        def _():
            block(buf.at[i - 1], False)

        return carry

    lax.fori_loop(1, 16, step, 0)

    total = acc[...]
    part_a = total[:, 0:128] / total[:, 64:65]
    part_b = total[:, 128:384] / total[:, 320:321]
    both = jnp.concatenate([part_a, part_b], axis=1)
    for side in (0, 1):
        attx[side] = jnp.concatenate(
            [both[(2 * k + side) * 24 : (2 * k + side + 1) * 24] for k in range(8)], axis=0
        ).astype(BF)
    heads_over = pltpu.make_async_remote_copy(
        src_ref=attx.at[1 - c], dst_ref=attr, send_sem=misc_send.at[1], recv_sem=misc_recv.at[1],
        device_id=partner, device_id_type=MESH,
    )
    heads_over.start()
    weights_over.wait_recv()
    mine = attx[c]
    partial = jnp.dot(mine[:, 0:64], ow_ref[0:64], preferred_element_type=F32)
    partial = partial + jnp.dot(mine[:, 128:320], ow_ref[64:256], preferred_element_type=F32)
    heads_over.wait_recv()
    given = attr[...]
    partial = partial + jnp.dot(given[:, 0:64], owp[0:64], preferred_element_type=F32)
    partial = partial + jnp.dot(given[:, 128:320], owp[64:256], preferred_element_type=F32)
    part[...] = partial.reshape(8, 24, 2048)

    sent = []

    def pass_on(src, dst, sign, k):
        way = 0 if sign == 1 else 1
        copy = pltpu.make_async_remote_copy(
            src_ref=src, dst_ref=dst, send_sem=z_send.at[way, k], recv_sem=z_recv.at[way, k],
            device_id=along_z(sign), device_id_type=MESH,
        )
        copy.start()
        sent.append(copy)
        return copy

    ways = ((1, 0, slice(0, 1024)), (-1, 1, slice(1024, 2048)))
    pending = {}
    for sign, way, cols in ways:
        far_out[way] = part[(z + 4) % 8, :, cols].astype(BF)
        pending[sign] = pass_on(far_out.at[way], far_in.at[way], sign, 0)
    for hop in (1, 2, 3):
        for sign, way, cols in ways:
            pending[sign].wait_recv()
            mine = part.at[(z + sign * (4 - hop) + 8) % 8]
            if hop == 1:
                inside = mine[:, cols] + far_in[way].astype(F32)
                outside = mine[:, 1024:2048] if way == 0 else mine[:, 0:1024]
                pair = [inside, outside] if way == 0 else [outside, inside]
                value = jnp.concatenate(pair, axis=1)
            else:
                value = mine[...] + step_in[way, hop - 2].astype(F32)
            step_out[way, hop - 1] = value.astype(BF)
            pending[sign] = pass_on(
                step_out.at[way, hop - 1], step_in.at[way, hop - 1], sign, hop
            )
    pending[1].wait_recv()
    pending[-1].wait_recv()
    out_ref[...] = part[z] + step_in[0, 2].astype(F32) + step_in[1, 2].astype(F32)

    ends = [(ring_send.at[k], size) for k, size in ring]
    ends += [(flip_send.at[k], HALF) for k in range(15)]
    for sem, size in ends:
        pltpu.make_async_remote_copy(
            src_ref=buf.at[0, pl.ds(0, size)], dst_ref=buf.at[0, pl.ds(0, size)],
            send_sem=sem, recv_sem=flip_recv.at[0], device_id=partner, device_id_type=MESH,
        ).wait_send()
    for copy in sent + [weights_over, heads_over]:
        copy.wait_send()


def head_sums(q_ext, own, wk, wv, ow, scale_one, scale_two):
    vmem = pl.BlockSpec(memory_space=pltpu.VMEM)
    return pl.pallas_call(
        functools.partial(attend_kernel, scale_one=scale_one, scale_two=scale_two),
        out_shape=jax.ShapeDtypeStruct((24, 2048), F32),
        in_specs=[vmem] * 5,
        out_specs=vmem,
        scratch_shapes=[
            pltpu.VMEM((15, 416, 512), BF),
            pltpu.VMEM((128, 384), BF),
            pltpu.VMEM((256, 384), BF),
            pltpu.VMEM((384, 384), BF),
            pltpu.VMEM((384, 384), F32),
            pltpu.VMEM((2, 384, 128), F32),
            pltpu.VMEM((256, 2048), BF),
            pltpu.VMEM((2, 192, 384), BF),
            pltpu.VMEM((192, 384), BF),
            pltpu.VMEM((8, 24, 2048), F32),
            pltpu.VMEM((2, 24, 1024), BF),
            pltpu.VMEM((2, 24, 1024), BF),
            pltpu.VMEM((2, 3, 24, 2048), BF),
            pltpu.VMEM((2, 3, 24, 2048), BF),
            pltpu.SemaphoreType.DMA((20,)),
            pltpu.SemaphoreType.DMA((15, 2)),
            pltpu.SemaphoreType.DMA((15,)),
            pltpu.SemaphoreType.DMA((15,)),
            pltpu.SemaphoreType.DMA((2,)),
            pltpu.SemaphoreType.DMA((2,)),
            pltpu.SemaphoreType.DMA((2, 4)),
            pltpu.SemaphoreType.DMA((2, 4)),
        ],
        compiler_params=pltpu.CompilerParams(
            collective_id=0, has_side_effects=True, vmem_limit_bytes=60 * 1024 * 1024
        ),
        name="attend",
    )(q_ext, own, wk, wv, ow)


def in_blocks(value, dim, count):
    dims = value.shape
    pieces = value.reshape(*dims[:dim], count, dims[dim] // count, *dims[dim + 1 :])
    return jnp.moveaxis(pieces, dim, 0)


def sum_at_owner(value, axis, dim):
    pieces = in_blocks(value, dim, lax.axis_size(axis))
    arrived = lax.all_to_all(pieces, axis, split_axis=0, concat_axis=0, tiled=True)
    return arrived.astype(jnp.float32).sum(axis=0)


def laid_out(pieces, dim):
    dims = list(pieces.shape[1:])
    dims[dim] *= pieces.shape[0]
    return jnp.moveaxis(pieces, 0, dim).reshape(dims)


def turned_blocks(pieces, axes, sequence):
    inside = pieces.shape[1:]
    out = pieces.reshape(*(lax.axis_size(a) for a in axes), *inside)
    for k in sequence:
        out = lax.all_to_all(out, axes[k], k, k, tiled=True)
    return out.reshape(-1, *inside)


def stepwise_exchange(value, axes, sequence, split_dim, concat_dim):
    pieces = in_blocks(value, split_dim, lax.axis_size(axes))
    return laid_out(turned_blocks(pieces, axes, sequence), concat_dim)


def angle_tables(places, rope_width):
    frequencies = rope_base ** (-jnp.arange(0, rope_width, 2, dtype=jnp.float32) / rope_width)
    angles = places[:, None] * frequencies[None, :]
    return (jnp.cos(angles), jnp.sin(angles))


def rope_turn(values, cosine, sine_table):
    half_size = values.shape[-1] // 2
    first_half = values[..., :half_size]
    second = values[..., half_size:]
    return jnp.concatenate(
        [first_half * cosine - second * sine_table, second * cosine + first_half * sine_table],
        axis=-1,
    )


def rms_scale(values, gain_vector):
    values = values.astype(jnp.float32)
    inverse = lax.rsqrt(jnp.mean(values * values, axis=-1, keepdims=True) + epsilon)
    return values * inverse * gain_vector


def slot_table(route_block, experts_all, capacity):
    flat_routes = route_block.reshape(-1)
    onehot = (flat_routes[:, None] == jnp.arange(experts_all, dtype=jnp.int32)[None, :]).astype(
        jnp.int32
    )
    rank_within = jnp.sum((jnp.cumsum(onehot, axis=0) - onehot) * onehot, axis=1)
    return flat_routes * capacity + rank_within


def local(
    residual,
    queries,
    query_rope,
    latent,
    key_rope,
    latent_gain,
    key_weight,
    value_weight,
    out_weight,
    norm_gain,
    routes,
    group_gate,
    expert_share,
    gate_weight,
    up_weight,
    down_weight,
):
    local_tokens = queries.shape[0]
    pair_dev = queries.shape[1]
    sp_count = lax.axis_size(SP)
    tp_count = lax.axis_size(TP)
    row_count = local_tokens // tp_count
    rope_width = key_rope.shape[1]
    first_place = lax.axis_index(SP) * local_tokens
    places = (first_place + jnp.arange(local_tokens, dtype=jnp.int32)).astype(jnp.float32)
    cosine, sine_table = angle_tables(places, rope_width)
    rotated_key = rope_turn(key_rope.astype(jnp.float32), cosine, sine_table).astype(jnp.bfloat16)
    turned = rope_turn(
        query_rope.astype(jnp.float32).reshape(local_tokens, pair_dev, 2, rope_width),
        cosine[:, None, None, :],
        sine_table[:, None, None, :],
    ).astype(jnp.bfloat16)
    compressed = rms_scale(latent, latent_gain).astype(BF)
    scale_one = (DK_A + rope_width) ** (-0.5)
    scale_two = (queries.shape[2] - DK_A + rope_width) ** (-0.5)
    own = jnp.concatenate(
        [jnp.pad(rotated_key.T, ((0, 0), (0, 128))), compressed], axis=0
    )
    flat = queries[:, 0]
    blank = jnp.zeros((local_tokens, 32), BF)
    q_ext = jnp.concatenate(
        [flat[:, :DK_A], turned[:, 0, 0], blank, flat[:, DK_A:], turned[:, 0, 1], blank], axis=1
    )
    key_flat = key_weight[:, 0].T
    value_flat = value_weight[:, 0]
    zeros = jnp.zeros((value_flat.shape[0], 64), BF)
    value_ext = jnp.concatenate(
        [value_flat[:, :DV_A], zeros, value_flat[:, DV_A:], zeros], axis=1
    )
    head_total = head_sums(
        q_ext, own, key_flat, value_ext, out_weight[0], scale_one, scale_two
    )
    mixed_rows = residual.astype(jnp.float32) + head_total
    normed = rms_scale(mixed_rows, norm_gain).astype(jnp.bfloat16)
    experts_dev = gate_weight.shape[0]
    experts_all = experts_dev * sp_count
    top_count = routes.shape[1]
    capacity = max(2, 3 * row_count * top_count // (2 * experts_all))
    slot_count = experts_all * capacity
    own_routes = lax.dynamic_slice_in_dim(routes, lax.axis_index(TP) * row_count, row_count, 0)
    own_slots = slot_table(own_routes, experts_all, capacity)
    pick_matrix = (jnp.arange(slot_count, dtype=jnp.int32)[:, None] == own_slots[None, :]).astype(
        jnp.bfloat16
    )
    pick_matrix = pick_matrix.reshape(slot_count, row_count, top_count).sum(axis=2)
    outgoing = (
        jnp.dot(pick_matrix, normed, preferred_element_type=jnp.float32)
        .astype(jnp.bfloat16)
        .reshape(sp_count, experts_dev, capacity, -1)
    )
    arrived = stepwise_exchange(outgoing, SP, (0, 1), 0, 0)
    gathered = lax.all_gather(arrived, TP, axis=0, tiled=True)
    gate_out = jnp.einsum(
        "secd,edf->secf", gathered, gate_weight, preferred_element_type=jnp.float32
    )
    up_out = jnp.einsum("secd,edf->secf", gathered, up_weight, preferred_element_type=jnp.float32)
    hidden = (jax.nn.silu(gate_out) * up_out).astype(jnp.bfloat16)
    expert_out = lax.psum_scatter(
        jnp.einsum(
            "secf,efd->secd", hidden, down_weight, preferred_element_type=jnp.float32
        ).astype(jnp.bfloat16),
        TP,
        scatter_dimension=0,
        tiled=True,
    )
    returned = lax.all_to_all(expert_out, SP, split_axis=0, concat_axis=0, tiled=True).reshape(
        slot_count, -1
    )
    selectors = (own_slots[:, None] == jnp.arange(slot_count, dtype=jnp.int32)[None, :]).astype(
        jnp.bfloat16
    )
    picked = jnp.dot(selectors, returned, preferred_element_type=jnp.float32).reshape(
        row_count, top_count, -1
    )
    route_weight = group_gate[:, None] * expert_share / jnp.sum(expert_share, axis=1, keepdims=True)
    expert_mix = jnp.sum(route_weight[:, :, None] * picked, axis=1)
    return (mixed_rows + expert_mix).astype(jnp.bfloat16)


def solution(mesh):
    finer = Mesh(mesh.devices.reshape(4, 4, 8, 2), ("y", "x", "z", "c"))
    placed = (
        P(SP_TP, None),
        P(SP, TP, None),
        P(SP, TP, None),
        P(SP, None),
        P(SP, None),
        P(),
        P(None, TP, None),
        P(None, TP, None),
        P(TP, None, None),
        P(),
        P(SP, None),
        P(SP_TP),
        P(SP_TP, None),
        P(SP, None, TP),
        P(SP, None, TP),
        P(SP, TP, None),
    )
    return jax.shard_map(
        local, mesh=finer, in_specs=placed, out_specs=P(SP_TP, None), check_vma=False
    )
```

time: 418 us -> 243 us (0.58)
  blocking collectives: 137 us -> 27.3 us
  waiting for transfers between devices: 185 us -> 107 us
  Pallas kernels: 0 us -> 56.4 us
  matrix products: 28.7 us -> 12.9 us
  loops' own time: 11.4 us -> 0 us
  starting transfers between devices: 14.7 us -> 7.32 us
  local copies, waits for them, and re-layouts: 16.9 us -> 11.6 us
    all_to_all x2, blocking collectives: 113 us -> 27.3 us  [turned_blocks(): out = lax.all_to_all(out, axes[k], k, k, tiled=True)]
    pallas_call x0 -> x1, Pallas kernels: none -> 56.4 us  [head_sums(): pl.pallas_call(functools.partial(attend_kernel, scale_one=scale_one, scal...]
    all_gather x2 -> x1, waiting for transfers between devices: 78.8 us -> 37.9 us  [local(): gathered = lax.all_gather(arrived, TP, axis=0, tiled=True)]
    all_to_all x1 -> x0, waiting for transfers between devices: 36.3 us -> none  [sum_at_owner(): lax.all_to_all(pieces, axis, split_axis=0, concat_axis=0, tiled=True)]
    all_gather x1 -> x0, blocking collectives: 24.3 us -> none  [local(): lax.all_gather(rotated_key, SP, axis=0, tiled=True)]
    dot_general x17 -> x0, matrix products: 15.5 us -> none  [the longest x4 4.51 us: online_step(): jnp.einsum('qhd,kd->hqk', query_turned, piece_rope, preferred_element_typ...]
    another operation x17 -> x0, loops' own time: 11.4 us -> none  [the longest x1 10.9 us: local(): lax.scan(one_block, carried, jnp.arange(blocks, dtype=jnp.int32))]
    dynamic_slice x17 -> x1, local copies, waits for them, and re-layouts: 10.5 us -> 0.76 us  [local(): lax.dynamic_slice_in_dim(routes, lax.axis_index(TP) * row_count, row_coun...]
  transfers between devices with their start and end apart: 5 -> 3, of which waited for: 5 -> 3; matrix products, arithmetic and copies ran while one was open for 1% -> 0% of each run, Pallas kernels for 0% -> 0%
where the time goes in v1:
time: 243 us
  waiting for transfers between devices  107 us (44%)
  Pallas kernels  56.4 us (23%)
  blocking collectives  27.3 us (11%)
  between operations  13.6 us (6%)
  matrix products  12.9 us (5%)
  local copies, waits for them, and re-layouts  11.6 us (5%)
  starting transfers between devices  7.32 us (3%)
  other arithmetic  6.01 us (2%)
    reduce_scatter x1, waiting for transfers between devices, local(): lax.psum_scatter(jnp.einsum('secf,efd->secd', hidden, down_weight, prefer...  62.1 us
    pallas_call x1, Pallas kernels, head_sums(): pl.pallas_call(functools.partial(attend_kernel, scale_one=scale_one, scal...  56.4 us
    all_gather x1, waiting for transfers between devices, local(): gathered = lax.all_gather(arrived, TP, axis=0, tiled=True)  37.9 us
    all_to_all x2, blocking collectives, turned_blocks(): out = lax.all_to_all(out, axes[k], k, k, tiled=True)  27.3 us
    dot_general x1, matrix products, local(): jnp.einsum('secf,efd->secd', hidden, down_weight, preferred_element_type=...  7.34 us
    all_to_all x1, waiting for transfers between devices, local(): lax.all_to_all(expert_out, SP, split_axis=0, concat_axis=0, tiled=True)  7.28 us
    all_to_all x1, starting transfers between devices, local(): lax.all_to_all(expert_out, SP, split_axis=0, concat_axis=0, tiled=True)  7.27 us
  transfers between devices with their start and end apart: 3, of which 3 were waited for; matrix products, arithmetic and copies ran while one was open for 0% of the time, Pallas kernels for 0%

profile of v1, /device:TPU:2, one launch (start us, length us, event | category | flops | bytes accessed | tf_op | source)
XLA Modules:
  0.0 242.6 jit_solution(11524813144417440906)
XLA Ops:
  6.5 0.0 copy-start
  6.5 0.0 copy-start.2
  6.5 0.0 copy-start.6
  6.5 0.0 all-gather.2.cloned.1.call-start
  6.6 1.2 slice.45
  7.8 0.9 slice.40
  8.7 1.1 slice.49
  9.8 0.9 slice.48
  10.7 0.7 convert_element_type.62
  11.5 0.8 convert.18
  12.3 0.2 subtract_convert_fusion.1
  12.5 0.1 copy.54
  12.6 0.1 copy.55
  12.7 0.0 copy-done.2
  12.7 0.2 fusion.21
  12.9 1.8 copy.43
  14.7 0.0 copy-done.6
  14.7 0.2 fusion.23
  14.9 0.8 fusion.25.own_ref
  15.7 0.0 copy-start.3
  15.7 0.9 pad_maximum_fusion.wv_ref
  16.6 0.0 copy-start.4
  16.7 0.9 concatenate.26.q_ref
  17.6 56.4 %attend.1 = f32[24,2048]{1,0:T(8,128)} custom-call(bf16[384,384]{1,0:T(8,128)(2,1)} %concatenate.26.q_ref, bf16[416,512]{1,0:T(8,128)(2,1)} %fusion.25.own_ref, bf16[256,512]{1,0:T(8,128)(2,1)} %bitcast.59, bf16[512,384]{1,0:T(8,128)(2,1)} %pad_maximum_fusion.wv_ref, bf16[256,2048]{1,0:T(8,128)(2,1)} %bitcast.60), custom_call_target="tpu_custom_call" | custom-call | tf_op jit(solution)/shard_map/attend/pallas_call | solution.py:339
  74.0 0.0 copy-done.3
  74.0 1.1 multiply_reduce_fusion
  75.1 0.8 constant_dynamic-slice_fusion
  75.8 0.1 copy.56
  75.9 0.1 eq.58
  76.0 0.1 fusion.29
  76.1 0.1 reduce_window_sum.11
  76.2 0.2 select_reduce_fusion
  76.4 0.1 reduce_sum.62
  76.5 0.1 copy.45
  76.6 0.1 fusion.33
  76.6 0.0 copy-done.4
  76.6 1.2 convolution_convert_fusion
  77.9 0.2 reshape_reshape_reshape.3
  78.1 15.4 %all_to_all.15 = bf16[4,4,1,2,2,2048]{5,4,3,1,2,0:T(2,128)(2,1)S(1)} all-to-all(bf16[4,4,1,2,2,2048]{5,4,3,1,2,0:T(2,128)(2,1)S(1)} %bitcast.61), channel_id=1, replica_groups=mesh['y'=4,'x'=4,'z'=8,'c'=2] {'y'}, dimensions={0} | all-to-all | bytes 524288 | tf_op jit(solution)/shard_map/all_to_all | solution.py:397
  93.5 0.2 copy.48
  93.7 11.8 %all_to_all.16 = bf16[4,4,1,2,2,2048]{5,4,3,0,2,1:T(2,128)(2,1)S(1)} all-to-all(bf16[4,4,1,2,2,2048]{5,4,3,0,2,1:T(2,128)(2,1)S(1)} %copy.48), channel_id=1, replica_groups=mesh['y'=4,'x'=4,'z'=8,'c'=2] {'x'}, dimensions={1} | all-to-all | bytes 524288 | tf_op jit(solution)/shard_map/all_to_all | solution.py:397
  105.5 0.2 copy.49
  105.7 0.8 reshape_reshape.3
  106.5 0.0 all-gather.2.cloned.1.call-update
  106.5 0.0 reduce-scatter.2.cloned.1.call-start
  106.6 37.9 %all-gather.2.cloned.1.call-done = bf16[256,2,2,2048]{3,0,2,1:T(8,128)(2,1)} async-done(((bf16[16,2,2,2048]{3,0,2,1:T(8,128)(2,1)}), bf16[256,2,2,2048]{3,0,2,1:T(8,128)(2,1)}) %all-gather.2.cloned.1.call-update) | async-done | bytes 4194320 | tf_op jit(solution)/shard_map/all_gather | solution.py:509
  144.5 4.1 %fusion.5 = f32[256,2,2,256]{3,0,2,1:T(8,128)S(1)} fusion(bf16[256,2,2,2048]{3,0,2,1:T(8,128)(2,1)} %all-gather.2.cloned.1.call-done, bf16[2,2048,256]{2,1,0:T(8,128)(2,1)} %param.29), kind=kOutput, calls=%fused_computation.8 | convolution fusion | flops 1073741824 | bytes 7340032 | tf_op jit(solution)/shard_map/secd,edf->secf/dot_general | solution.py:510
  148.6 0.0 copy-done
  148.6 7.3 %convert_bitcast_fusion = bf16[256,2,2,2048]{3,0,2,1:T(8,128)(2,1)} fusion(bf16[2,256,2048]{2,1,0:T(8,128)(2,1)S(1)} %copy-done, bf16[256,2,2,2048]{3,0,2,1:T(8,128)(2,1)} %all-gather.2.cloned.1.call-done, bf16[2,2048,256]{2,1,0:T(8,128)(2,1)} %param.30, f32[256,2,2,256]{3,0,2,1:T(8,128)S(1)} %fusion.5), kind=kOutput, calls=%fused_computation | convolution fusion | flops 2151153664 | bytes 13631488 | tf_op jit(solution)/shard_map/secf,efd->secd/dot_general | solution.py:516
  156.0 0.0 copy-start.5
  156.0 0.0 copy-start.7
  156.0 0.0 copy-start.1
  156.0 0.0 reduce-scatter.2.cloned.1.call-update
  156.0 62.1 %reduce-scatter.2.cloned.1.call-done = bf16[16,2,2,2048]{3,0,2,1:T(8,128)(2,1)} async-done(((bf16[256,2,2,2048]{3,0,2,1:T(8,128)(2,1)}), bf16[16,2,2,2048]{3,0,2,1:T(8,128)(2,1)}) %reduce-scatter.2.cloned.1.call-update) | async-done | bytes 262160 | tf_op jit(solution)/shard_map/reduce_scatter | solution.py:515
  218.2 1.9 copy.50
  220.1 7.3 %all-to-all-start.2 = ((bf16[16,2,2,2048]{3,2,1,0:T(2,128)(2,1)}), bf16[16,2,2,2048]{3,2,1,0:T(2,128)(2,1)S(1)}, u32[]{:S(2)}, u32[]{:S(2)}) async-start(bf16[16,2,2,2048]{3,2,1,0:T(2,128)(2,1)} %copy.50), calls=%async_computation.3 | async-start | bytes 524288 | tf_op jit(solution)/shard_map/all_to_all | solution.py:523
  227.4 0.0 copy-done.5
  227.4 0.0 copy-done.7
  227.4 7.3 %all-to-all-done.2 = bf16[16,2,2,2048]{3,2,1,0:T(2,128)(2,1)S(1)} async-done(((bf16[16,2,2,2048]{3,2,1,0:T(2,128)(2,1)}), bf16[16,2,2,2048]{3,2,1,0:T(2,128)(2,1)S(1)}, u32[]{:S(2)}, u32[]{:S(2)}) %all-to-all-start.2) | async-done | bytes 262176 | tf_op jit(solution)/shard_map/all_to_all | solution.py:523
  234.7 0.1 reshape.180
  234.8 0.3 fusion.17
  235.0 0.0 copy-done.1
  235.1 0.7 add_convert_fusion
  (12 shorter events, 0.1 us)
Async XLA Ops:
  6.5 142.1 %copy-start = (bf16[2,256,2048]{2,1,0:T(8,128)(2,1)S(1)}, bf16[2,256,2048]{2,1,0:T(8,128)(2,1)}, u32[]{:S(2)}) copy-start(bf16[2,256,2048]{2,1,0:T(8,128)(2,1)} %param.31) | copy-start | bytes 6291460
  6.5 6.2 %copy-start.2 = (bf16[384,512]{1,0:T(8,128)(2,1)S(1)}, bf16[384,512]{1,0:T(8,128)(2,1)}, u32[]{:S(2)}) copy-start(bf16[384,512]{1,0:T(8,128)(2,1)} %param.19) | copy-start | bytes 1179652
  6.5 8.2 %copy-start.6 = (f32[512]{0:T(512)S(1)}, f32[512]{0:T(512)}, u32[]{:S(2)}) copy-start(f32[512]{0:T(512)} %param.21) | copy-start | bytes 6148
  6.5 138.0 %all-gather.2.cloned.1.call-start = ((), (), s32[]{:S(2)}) async-start(), calls=%async_computation.4 | async-start | bytes 4456448 | tf_op jit(solution)/shard_map/all_gather | solution.py:509
  15.7 58.3 %copy-start.3 = (bf16[24,2048]{1,0:T(8,128)(2,1)S(1)}, bf16[24,2048]{1,0:T(8,128)(2,1)}, u32[]{:S(2)}) copy-start(bf16[24,2048]{1,0:T(8,128)(2,1)} %param.16) | copy-start | bytes 294916
  16.6 60.0 %copy-start.4 = (f32[2048]{0:T(1024)S(1)}, f32[2048]{0:T(1024)}, u32[]{:S(2)}) copy-start(f32[2048]{0:T(1024)} %param.25) | copy-start | bytes 24580
  106.5 111.6 %reduce-scatter.2.cloned.1.call-start = ((), (), s32[]{:S(2)}) async-start(), calls=%async_computation.5 | async-start | bytes 4456448 | tf_op jit(solution)/shard_map/reduce_scatter | solution.py:515
  156.0 71.4 %copy-start.5 = (f32[24,2]{0,1:T(2,128)S(1)}, f32[24,2]{0,1:T(2,128)}, u32[]{:S(2)}) copy-start(f32[24,2]{0,1:T(2,128)} %param.28) | copy-start | bytes 580
  156.0 71.4 %copy-start.7 = (f32[24]{0:T(128)S(1)}, f32[24]{0:T(128)}, u32[]{:S(2)}) copy-start(f32[24]{0:T(128)} %param.27) | copy-start | bytes 292
  156.0 79.1 %copy-start.1 = (f32[24,2048]{1,0:T(8,128)S(1)}, f32[24,2048]{1,0:T(8,128)}, u32[]{:S(2)}) copy-start(f32[24,2048]{1,0:T(8,128)} %attend.1) | copy-start | bytes 589828
  220.1 14.6 %all-to-all-start.2 = ((bf16[16,2,2,2048]{3,2,1,0:T(2,128)(2,1)}), bf16[16,2,2,2048]{3,2,1,0:T(2,128)(2,1)S(1)}, u32[]{:S(2)}, u32[]{:S(2)}) async-start(bf16[16,2,2,2048]{3,2,1,0:T(2,128)(2,1)} %copy.50), calls=%async_computation.3 | async-start | bytes 524288 | tf_op jit(solution)/shard_map/all_to_all | solution.py:523
Sparse Core Ops, SparseCore 0:
  106.6 37.8 all-gather.1
  156.1 61.9 reduce-scatter.1

commit v2 on v1

--- a/solution.py
+++ b/solution.py
@@ -46,11 +46,27 @@
     pl.semaphore_wait(barrier, len(devices))
 
 
-def attend_kernel(
-    q_ref, own_ref, wk_ref, wv_ref, ow_ref, out_ref,
-    buf, kta, ktb, vx, acc, top, owp, attx, attr, part,
-    far_out, far_in, step_out, step_in,
-    ring_send, ring_recv, flip_send, flip_recv, misc_send, misc_recv, z_send, z_recv,
+DZ = (0, -1, 1, -2, 2, -3, 3, 4)
+BASE = {dz: 2 * k for k, dz in enumerate(DZ)}
+
+
+def spread_place(column):
+    return column + jnp.where(column >= DK_A, 64, 0)
+
+
+def chosen(condition):
+    return jnp.where(condition, 1.0, 0.0).astype(BF)
+
+
+def layer_kernel(
+    q_ref, turned_ref, own_ref, wk_ref, wv_ref, ow_ref, residual_ref, gain_ref,
+    slots_ref, spots_ref, share_ref, gate_hbm, up_hbm, down_hbm, out_ref,
+    qx, wkt, wvx, buf, kta, ktb, vx, acc, top, owp, attx, attr, part,
+    far_out, far_in, step_out, step_in, mixed_ref, disp, arr, rows_ref,
+    held, gate, up, down, made, given, rs_out, rs_in, sums_ref, ret, back,
+    ring_send, ring_recv, flip_send, flip_recv, misc_send, misc_recv, head_send, head_recv,
+    disp_send, disp_recv, load_sem, z_send, z_recv, swap_send, swap_recv,
+    give_send, give_recv, rs_send, rs_recv, back_send, back_recv,
     *, scale_one, scale_two,
 ):
     y, x, z, c = place()
@@ -70,9 +86,18 @@
         second = SLOT[(da % 4, db % 4)]
         return first if first == second else first + c * (second - first)
 
-    meet(
-        [partner, along_a(1), along_a(-1), along_b(1), along_b(-1), along_z(1), along_z(-1)]
-    )
+    me = y * 4 + x
+    peers = [
+        (dy, dx, ((y + dy) % 4, (x + dx) % 4, z, c))
+        for dy in range(4) for dx in range(4) if dy or dx
+    ]
+    loads = [
+        pltpu.make_async_copy(src, dst, load_sem.at[k])
+        for k, (src, dst) in enumerate(((gate_hbm, gate), (up_hbm, up), (down_hbm, down)))
+    ]
+    for load in loads:
+        load.start()
+    meet([partner, along_z(1), along_z(-1)] + [peer[2] for peer in peers])
     start_row = c * HALF
     other_row = (1 - c) * HALF
     counts = {"ring": 0}
@@ -140,6 +165,27 @@
     )
     weights_over.start()
 
+    spread = chosen(
+        lax.broadcasted_iota(jnp.int32, (256, 384), 1)
+        == spread_place(lax.broadcasted_iota(jnp.int32, (256, 384), 0))
+    )
+    turns = lax.broadcasted_iota(jnp.int32, (64, 384), 0)
+    turns = chosen(
+        lax.broadcasted_iota(jnp.int32, (64, 384), 1)
+        == turns + 64 + jnp.where(turns >= 32, 224, 0)
+    )
+    qx[...] = (
+        jnp.dot(q_ref[...], spread, preferred_element_type=F32)
+        + jnp.dot(turned_ref[...], turns, preferred_element_type=F32)
+    ).astype(BF)
+    wvx[...] = jnp.dot(wv_ref[...], spread, preferred_element_type=F32).astype(BF)
+    unit = chosen(
+        lax.broadcasted_iota(jnp.int32, (256, 256), 0)
+        == lax.broadcasted_iota(jnp.int32, (256, 256), 1)
+    )
+    wkt[...] = lax.dot_general(
+        unit, wk_ref[...], (((1,), (1,)), ((), ())), preferred_element_type=F32
+    ).astype(BF)
     kta[96:128] = jnp.zeros((32, 384), BF)
     ktb[224:256] = jnp.zeros((32, 384), BF)
     lanes = lax.broadcasted_iota(jnp.int32, (1, 384), 1)
@@ -153,15 +199,15 @@
         rope = ref[0:32, 0:384]
         lat = ref[32:416, :]
         keys = lax.dot_general(
-            wk_ref[...], lat, (((1,), (1,)), ((), ())), preferred_element_type=F32
+            wkt[...], lat, (((1,), (1,)), ((), ())), preferred_element_type=F32
         ).astype(BF)
         kta[0:64] = keys[0:64]
         kta[64:96] = rope
         ktb[0:192] = keys[64:256]
         ktb[192:224] = rope
-        vx[...] = (jnp.dot(lat, wv_ref[...], preferred_element_type=F32) + ones).astype(BF)
+        vx[...] = (jnp.dot(lat, wvx[...], preferred_element_type=F32) + ones).astype(BF)
         for cols, keys_ref, h, factor in heads:
-            scores = jnp.dot(q_ref[:, cols], keys_ref[...], preferred_element_type=F32)
+            scores = jnp.dot(qx[:, cols], keys_ref[...], preferred_element_type=F32)
             if first:
                 rows = lax.broadcasted_iota(jnp.int32, (384, 384), 0)
                 places = lax.broadcasted_iota(jnp.int32, (384, 384), 1)
@@ -186,8 +232,6 @@
 
     block(own_ref, True)
 
-    me = y * 4 + x
-
     def step(i, carry):
         @pl.when(i == 1)
         def _():
@@ -282,9 +326,9 @@
     partial = jnp.dot(mine[:, 0:64], ow_ref[0:64], preferred_element_type=F32)
     partial = partial + jnp.dot(mine[:, 128:320], ow_ref[64:256], preferred_element_type=F32)
     heads_over.wait_recv()
-    given = attr[...]
-    partial = partial + jnp.dot(given[:, 0:64], owp[0:64], preferred_element_type=F32)
-    partial = partial + jnp.dot(given[:, 128:320], owp[64:256], preferred_element_type=F32)
+    theirs = attr[...]
+    partial = partial + jnp.dot(theirs[:, 0:64], owp[0:64], preferred_element_type=F32)
+    partial = partial + jnp.dot(theirs[:, 128:320], owp[64:256], preferred_element_type=F32)
     part[...] = partial.reshape(8, 24, 2048)
 
     sent = []
@@ -292,7 +336,7 @@
     def pass_on(src, dst, sign, k):
         way = 0 if sign == 1 else 1
         copy = pltpu.make_async_remote_copy(
-            src_ref=src, dst_ref=dst, send_sem=z_send.at[way, k], recv_sem=z_recv.at[way, k],
+            src_ref=src, dst_ref=dst, send_sem=head_send.at[way, k], recv_sem=head_recv.at[way, k],
             device_id=along_z(sign), device_id_type=MESH,
         )
         copy.start()
@@ -321,8 +365,183 @@
             )
     pending[1].wait_recv()
     pending[-1].wait_recv()
-    out_ref[...] = part[z] + step_in[0, 2].astype(F32) + step_in[1, 2].astype(F32)
-
+    mixed = residual_ref[...].astype(F32) + part[z]
+    mixed = mixed + step_in[0, 2].astype(F32) + step_in[1, 2].astype(F32)
+    mixed_ref[...] = mixed
+    inverse = lax.rsqrt(jnp.mean(mixed * mixed, axis=1, keepdims=True) + epsilon)
+    normed = mixed * inverse * gain_ref[...]
+    stack = jnp.concatenate([normed[:, j * 512 : (j + 1) * 512] for j in range(4)], axis=0)
+    rows = lax.broadcasted_iota(jnp.int32, (256, 96), 0)
+    columns = lax.broadcasted_iota(jnp.int32, (256, 96), 1)
+    wanted = (rows // 16) * 4 + rows % 4
+    hit = (wanted == slots_ref[0:1, :]) | (wanted == slots_ref[1:2, :])
+    pick = chosen(hit & ((rows // 4) % 4 == columns // 24))
+    outgoing = jnp.dot(pick, stack.astype(BF), preferred_element_type=F32).astype(BF)
+    disp[...] = outgoing.reshape(16, 16, 512)
+
+    def exchange(source, target, send_sem, recv_sem):
+        target[me] = source[me]
+        moves = []
+        for dy, dx, peer in peers:
+            there = peer[0] * 4 + peer[1]
+            k = dy * 4 + dx - 1
+            copy = pltpu.make_async_remote_copy(
+                src_ref=source.at[there], dst_ref=target.at[me],
+                send_sem=send_sem.at[k], recv_sem=recv_sem.at[k],
+                device_id=peer, device_id_type=MESH,
+            )
+            copy.start()
+            moves.append(copy)
+        for copy in moves:
+            copy.wait_recv()
+        return moves
+
+    moves = exchange(disp, arr, disp_send, disp_recv)
+    order = lax.broadcasted_iota(jnp.int32, (256, 256), 0)
+    order = ((order // 2) % 16) * 16 + (order // 64) * 4 + ((order // 32) % 2) * 2 + order % 2
+    unpack = chosen(lax.broadcasted_iota(jnp.int32, (256, 256), 1) == order)
+    arrived_rows = jnp.dot(
+        unpack, arr[...].reshape(256, 512), preferred_element_type=F32
+    ).astype(BF)
+    for j in range(4):
+        piece_rows = arrived_rows[j * 64 : (j + 1) * 64].reshape(2, 32, 512)
+        rows_ref[:, :, j * 512 : (j + 1) * 512] = piece_rows
+
+    copies = []
+
+    def remote(src, dst, send_sem, recv_sem, device):
+        copy = pltpu.make_async_remote_copy(
+            src_ref=src, dst_ref=dst, send_sem=send_sem, recv_sem=recv_sem,
+            device_id=device, device_id_type=MESH,
+        )
+        copy.start()
+        copies.append(copy)
+        return copy
+
+    hops = {}
+    flips = {}
+    for e in (0, 1):
+        for way, sign in ((0, 1), (1, -1)):
+            hops[way, 1, e] = remote(
+                rows_ref.at[e], held.at[e, BASE[-sign] + c],
+                z_send.at[way, 0, e], z_recv.at[way, 0, e], along_z(sign),
+            )
+        flips[0, e] = remote(
+            rows_ref.at[e], held.at[e, c], swap_send.at[0, e], swap_recv.at[0, e], partner
+        )
+        held[e, c] = rows_ref[e]
+
+    def compute(first, count, dzs):
+        for e in (0, 1):
+            rows = held[e, first : first + count].reshape(count * 32, 2048)
+            inner = jnp.dot(rows, gate[e], preferred_element_type=F32)
+            inner = inner / (1.0 + jnp.exp(-inner))
+            inner = inner * jnp.dot(rows, up[e], preferred_element_type=F32)
+            result = jnp.dot(inner.astype(BF), down[e], preferred_element_type=F32)
+            made[e, first : first + count] = result.astype(BF).reshape(count, 32, 2048)
+            for dz in dzs:
+                k = BASE[dz] // 2
+                gives[dz, e] = remote(
+                    made.at[e, BASE[dz] + 1 - c], given.at[e, k],
+                    give_send.at[k, e], give_recv.at[k, e], partner,
+                )
+
+    gives = {}
+
+    def chip_sum(dz, e):
+        if (dz, e) in gives:
+            gives.pop((dz, e)).wait_recv()
+        return made[e, BASE[dz] + c].astype(F32) + given[e, BASE[dz] // 2].astype(F32)
+
+    for load in loads:
+        load.wait()
+    for e in (0, 1):
+        flips[0, e].wait_recv()
+    compute(0, 2, (0,))
+    for dist in (1, 2, 3):
+        for e in (0, 1):
+            for way, sign in ((0, 1), (1, -1)):
+                hops[way, dist, e].wait_recv()
+                dz = -sign * dist
+                spot = held.at[e, BASE[dz] + c]
+                k = BASE[dz] // 2
+                if dist < 3:
+                    target = held.at[e, BASE[dz - sign] + c]
+                elif way == e:
+                    target = held.at[e, BASE[4] + c]
+                else:
+                    target = None
+                if target is not None:
+                    hops[way, dist + 1, e] = remote(
+                        spot, target, z_send.at[way, dist, e], z_recv.at[way, dist, e],
+                        along_z(sign),
+                    )
+                flips[k, e] = remote(
+                    spot, spot, swap_send.at[k, e], swap_recv.at[k, e], partner
+                )
+        for e in (0, 1):
+            for dz in (-dist, dist):
+                flips[BASE[dz] // 2, e].wait_recv()
+        compute(4 * dist - 2, 4, (-dist, dist))
+
+    sums = {}
+
+    def push(way, e, hop, value):
+        sign = 1 if way == 0 else -1
+        rs_out[way, e, hop] = value.astype(BF)
+        sums[way, e] = remote(
+            rs_out.at[way, e, hop], rs_in.at[way, e, hop],
+            rs_send.at[way, e, hop], rs_recv.at[way, e, hop], along_z(sign),
+        )
+
+    push(0, 1, 1, chip_sum(3, 1))
+    push(1, 0, 1, chip_sum(-3, 0))
+    for e in (0, 1):
+        hops[e, 4, e].wait_recv()
+        spot = held.at[e, BASE[4] + c]
+        flips[7, e] = remote(spot, spot, swap_send.at[7, e], swap_recv.at[7, e], partner)
+    for e in (0, 1):
+        flips[7, e].wait_recv()
+    compute(14, 2, (4,))
+    push(0, 0, 0, chip_sum(4, 0))
+    push(1, 1, 0, chip_sum(4, 1))
+    for hop in (1, 2, 3):
+        if hop < 3:
+            for way, e in ((0, 1), (1, 0)):
+                sums[way, e].wait_recv()
+                dz = (3 - hop) * (1 if way == 0 else -1)
+                push(way, e, hop + 1, chip_sum(dz, e) + rs_in[way, e, hop].astype(F32))
+        for way, e in ((0, 0), (1, 1)):
+            sums[way, e].wait_recv()
+            dz = (4 - hop) * (1 if way == 0 else -1)
+            push(way, e, hop, chip_sum(dz, e) + rs_in[way, e, hop - 1].astype(F32))
+    for e in (0, 1):
+        own = chip_sum(0, e)
+        for way in (0, 1):
+            sums[way, e].wait_recv()
+            own = own + rs_in[way, e, 3].astype(F32)
+        sums_ref[e] = own.astype(BF)
+    collected = jnp.concatenate(
+        [sums_ref[:, :, j * 512 : (j + 1) * 512].reshape(64, 512) for j in range(4)], axis=0
+    )
+    order = lax.broadcasted_iota(jnp.int32, (256, 256), 1)
+    order = ((order // 2) % 16) * 16 + (order // 64) * 4 + ((order // 32) % 2) * 2 + order % 2
+    repack = chosen(lax.broadcasted_iota(jnp.int32, (256, 256), 0) == order)
+    ret[...] = (
+        jnp.dot(repack, collected, preferred_element_type=F32).astype(BF).reshape(16, 16, 512)
+    )
+    moves += exchange(ret, back, back_send, back_recv)
+    returned = back[...].reshape(256, 512)
+    result = mixed_ref[...]
+    spots = lax.broadcasted_iota(jnp.int32, (96, 256), 1)
+    for k in (0, 1):
+        select = chosen(spots == spots_ref[:, k : k + 1])
+        picked = jnp.dot(select, returned, preferred_element_type=F32)
+        picked = jnp.concatenate([picked[j * 24 : (j + 1) * 24] for j in range(4)], axis=1)
+        result = result + share_ref[:, k : k + 1] * picked
+    out_ref[...] = result.astype(BF)
+    for copy in copies + moves:
+        copy.wait_send()
     ends = [(ring_send.at[k], size) for k, size in ring]
     ends += [(flip_send.at[k], HALF) for k in range(15)]
     for sem, size in ends:
@@ -334,14 +553,19 @@
         copy.wait_send()
 
 
-def head_sums(q_ext, own, wk, wv, ow, scale_one, scale_two):
+def layer(operands, weights, scale_one, scale_two):
     vmem = pl.BlockSpec(memory_space=pltpu.VMEM)
+    hbm = pl.BlockSpec(memory_space=pl.ANY)
+    dma = pltpu.SemaphoreType.DMA
     return pl.pallas_call(
-        functools.partial(attend_kernel, scale_one=scale_one, scale_two=scale_two),
-        out_shape=jax.ShapeDtypeStruct((24, 2048), F32),
-        in_specs=[vmem] * 5,
+        functools.partial(layer_kernel, scale_one=scale_one, scale_two=scale_two),
+        out_shape=jax.ShapeDtypeStruct((24, 2048), BF),
+        in_specs=[vmem] * len(operands) + [hbm] * len(weights),
         out_specs=vmem,
         scratch_shapes=[
+            pltpu.VMEM((384, 384), BF),
+            pltpu.VMEM((256, 512), BF),
+            pltpu.VMEM((512, 384), BF),
             pltpu.VMEM((15, 416, 512), BF),
             pltpu.VMEM((128, 384), BF),
             pltpu.VMEM((256, 384), BF),
@@ -356,51 +580,48 @@
             pltpu.VMEM((2, 24, 1024), BF),
             pltpu.VMEM((2, 3, 24, 2048), BF),
             pltpu.VMEM((2, 3, 24, 2048), BF),
-            pltpu.SemaphoreType.DMA((20,)),
-            pltpu.SemaphoreType.DMA((15, 2)),
-            pltpu.SemaphoreType.DMA((15,)),
-            pltpu.SemaphoreType.DMA((15,)),
-            pltpu.SemaphoreType.DMA((2,)),
-            pltpu.SemaphoreType.DMA((2,)),
-            pltpu.SemaphoreType.DMA((2, 4)),
-            pltpu.SemaphoreType.DMA((2, 4)),
+            pltpu.VMEM((24, 2048), F32),
+            pltpu.VMEM((16, 16, 512), BF),
+            pltpu.VMEM((16, 16, 512), BF),
+            pltpu.VMEM((2, 32, 2048), BF),
+            pltpu.VMEM((2, 16, 32, 2048), BF),
+            pltpu.VMEM((2, 2048, 256), BF),
+            pltpu.VMEM((2, 2048, 256), BF),
+            pltpu.VMEM((2, 256, 2048), BF),
+            pltpu.VMEM((2, 16, 32, 2048), BF),
+            pltpu.VMEM((2, 8, 32, 2048), BF),
+            pltpu.VMEM((2, 2, 4, 32, 2048), BF),
+            pltpu.VMEM((2, 2, 4, 32, 2048), BF),
+            pltpu.VMEM((2, 32, 2048), BF),
+            pltpu.VMEM((16, 16, 512), BF),
+            pltpu.VMEM((16, 16, 512), BF),
+            dma((20,)),
+            dma((15, 2)),
+            dma((15,)),
+            dma((15,)),
+            dma((2,)),
+            dma((2,)),
+            dma((2, 4)),
+            dma((2, 4)),
+            dma((15,)),
+            dma((15,)),
+            dma((3,)),
+            dma((2, 4, 2)),
+            dma((2, 4, 2)),
+            dma((8, 2)),
+            dma((8, 2)),
+            dma((8, 2)),
+            dma((8, 2)),
+            dma((2, 2, 4)),
+            dma((2, 2, 4)),
+            dma((15,)),
+            dma((15,)),
         ],
         compiler_params=pltpu.CompilerParams(
             collective_id=0, has_side_effects=True, vmem_limit_bytes=60 * 1024 * 1024
         ),
-        name="attend",
-    )(q_ext, own, wk, wv, ow)
-
-
-def in_blocks(value, dim, count):
-    dims = value.shape
-    pieces = value.reshape(*dims[:dim], count, dims[dim] // count, *dims[dim + 1 :])
-    return jnp.moveaxis(pieces, dim, 0)
-
-
-def sum_at_owner(value, axis, dim):
-    pieces = in_blocks(value, dim, lax.axis_size(axis))
-    arrived = lax.all_to_all(pieces, axis, split_axis=0, concat_axis=0, tiled=True)
-    return arrived.astype(jnp.float32).sum(axis=0)
-
-
-def laid_out(pieces, dim):
-    dims = list(pieces.shape[1:])
-    dims[dim] *= pieces.shape[0]
-    return jnp.moveaxis(pieces, 0, dim).reshape(dims)
-
-
-def turned_blocks(pieces, axes, sequence):
-    inside = pieces.shape[1:]
-    out = pieces.reshape(*(lax.axis_size(a) for a in axes), *inside)
-    for k in sequence:
-        out = lax.all_to_all(out, axes[k], k, k, tiled=True)
-    return out.reshape(-1, *inside)
-
-
-def stepwise_exchange(value, axes, sequence, split_dim, concat_dim):
-    pieces = in_blocks(value, split_dim, lax.axis_size(axes))
-    return laid_out(turned_blocks(pieces, axes, sequence), concat_dim)
+        name="layer",
+    )(*operands, *weights)
 
 
 def angle_tables(places, rope_width):
@@ -423,15 +644,6 @@
     values = values.astype(jnp.float32)
     inverse = lax.rsqrt(jnp.mean(values * values, axis=-1, keepdims=True) + epsilon)
     return values * inverse * gain_vector
-
-
-def slot_table(route_block, experts_all, capacity):
-    flat_routes = route_block.reshape(-1)
-    onehot = (flat_routes[:, None] == jnp.arange(experts_all, dtype=jnp.int32)[None, :]).astype(
-        jnp.int32
-    )
-    rank_within = jnp.sum((jnp.cumsum(onehot, axis=0) - onehot) * onehot, axis=1)
-    return flat_routes * capacity + rank_within
 
 
 def local(
@@ -454,7 +666,6 @@
 ):
     local_tokens = queries.shape[0]
     pair_dev = queries.shape[1]
-    sp_count = lax.axis_size(SP)
     tp_count = lax.axis_size(TP)
     row_count = local_tokens // tp_count
     rope_width = key_rope.shape[1]
@@ -474,64 +685,29 @@
         [jnp.pad(rotated_key.T, ((0, 0), (0, 128))), compressed], axis=0
     )
     flat = queries[:, 0]
-    blank = jnp.zeros((local_tokens, 32), BF)
-    q_ext = jnp.concatenate(
-        [flat[:, :DK_A], turned[:, 0, 0], blank, flat[:, DK_A:], turned[:, 0, 1], blank], axis=1
-    )
-    key_flat = key_weight[:, 0].T
-    value_flat = value_weight[:, 0]
-    zeros = jnp.zeros((value_flat.shape[0], 64), BF)
-    value_ext = jnp.concatenate(
-        [value_flat[:, :DV_A], zeros, value_flat[:, DV_A:], zeros], axis=1
-    )
-    head_total = head_sums(
-        q_ext, own, key_flat, value_ext, out_weight[0], scale_one, scale_two
-    )
-    mixed_rows = residual.astype(jnp.float32) + head_total
-    normed = rms_scale(mixed_rows, norm_gain).astype(jnp.bfloat16)
-    experts_dev = gate_weight.shape[0]
-    experts_all = experts_dev * sp_count
-    top_count = routes.shape[1]
-    capacity = max(2, 3 * row_count * top_count // (2 * experts_all))
-    slot_count = experts_all * capacity
     own_routes = lax.dynamic_slice_in_dim(routes, lax.axis_index(TP) * row_count, row_count, 0)
-    own_slots = slot_table(own_routes, experts_all, capacity)
-    pick_matrix = (jnp.arange(slot_count, dtype=jnp.int32)[:, None] == own_slots[None, :]).astype(
-        jnp.bfloat16
-    )
-    pick_matrix = pick_matrix.reshape(slot_count, row_count, top_count).sum(axis=2)
-    outgoing = (
-        jnp.dot(pick_matrix, normed, preferred_element_type=jnp.float32)
-        .astype(jnp.bfloat16)
-        .reshape(sp_count, experts_dev, capacity, -1)
-    )
-    arrived = stepwise_exchange(outgoing, SP, (0, 1), 0, 0)
-    gathered = lax.all_gather(arrived, TP, axis=0, tiled=True)
-    gate_out = jnp.einsum(
-        "secd,edf->secf", gathered, gate_weight, preferred_element_type=jnp.float32
-    )
-    up_out = jnp.einsum("secd,edf->secf", gathered, up_weight, preferred_element_type=jnp.float32)
-    hidden = (jax.nn.silu(gate_out) * up_out).astype(jnp.bfloat16)
-    expert_out = lax.psum_scatter(
-        jnp.einsum(
-            "secf,efd->secd", hidden, down_weight, preferred_element_type=jnp.float32
-        ).astype(jnp.bfloat16),
-        TP,
-        scatter_dimension=0,
-        tiled=True,
-    )
-    returned = lax.all_to_all(expert_out, SP, split_axis=0, concat_axis=0, tiled=True).reshape(
-        slot_count, -1
-    )
-    selectors = (own_slots[:, None] == jnp.arange(slot_count, dtype=jnp.int32)[None, :]).astype(
-        jnp.bfloat16
-    )
-    picked = jnp.dot(selectors, returned, preferred_element_type=jnp.float32).reshape(
-        row_count, top_count, -1
-    )
+    choices = own_routes.reshape(-1)
+    order = jnp.arange(choices.shape[0], dtype=jnp.int32)
+    same = (choices[:, None] == choices[None, :]) & (order[:, None] > order[None, :])
+    slots = (choices * 2 + jnp.sum(same.astype(jnp.int32), axis=1)).reshape(row_count, 2)
+    spots = (slots // 4) * 16 + slots % 4
+    quarters = jnp.arange(4, dtype=jnp.int32)
+    spots = (spots[None] + 4 * quarters[:, None, None]).reshape(4 * row_count, 2)
     route_weight = group_gate[:, None] * expert_share / jnp.sum(expert_share, axis=1, keepdims=True)
-    expert_mix = jnp.sum(route_weight[:, :, None] * picked, axis=1)
-    return (mixed_rows + expert_mix).astype(jnp.bfloat16)
+    operands = (
+        flat,
+        turned.reshape(local_tokens, 2 * rope_width),
+        own,
+        key_weight[:, 0],
+        value_weight[:, 0],
+        out_weight[0],
+        residual,
+        norm_gain[None],
+        jnp.tile(slots.T, (1, 4)),
+        spots,
+        route_weight,
+    )
+    return layer(operands, (gate_weight, up_weight, down_weight), scale_one, scale_two)
 
 
 def solution(mesh):

time: 243 us -> 137 us (0.56)
  waiting for transfers between devices: 107 us -> 0 us
  Pallas kernels: 56.4 us -> 125 us
  blocking collectives: 27.3 us -> 0 us
  between operations: 13.6 us -> 0.08 us
  matrix products: 12.9 us -> 0 us
  local copies, waits for them, and re-layouts: 11.6 us -> 3.65 us
  starting transfers between devices: 7.32 us -> 0 us
    pallas_call x1, Pallas kernels: 56.4 us -> 125 us  [layer(): pl.pallas_call(functools.partial(layer_kernel, scale_one=scale_one, scale...]
    reduce_scatter x1 -> x0, waiting for transfers between devices: 62.1 us -> none  [local(): lax.psum_scatter(jnp.einsum('secf,efd->secd', hidden, down_weight, prefer...]
    all_gather x1 -> x0, waiting for transfers between devices: 37.9 us -> none  [local(): gathered = lax.all_gather(arrived, TP, axis=0, tiled=True)]
    all_to_all x2 -> x0, blocking collectives: 27.3 us -> none  [turned_blocks(): out = lax.all_to_all(out, axes[k], k, k, tiled=True)]
    dot_general x4 -> x0, matrix products: 12.9 us -> none  [the longest x1 7.34 us: local(): jnp.einsum('secf,efd->secd', hidden, down_weight, preferred_element_type=...]
    all_to_all x1 -> x0, waiting for transfers between devices: 7.28 us -> none  [local(): lax.all_to_all(expert_out, SP, split_axis=0, concat_axis=0, tiled=True)]
    all_to_all x1 -> x0, starting transfers between devices: 7.27 us -> none  [local(): lax.all_to_all(expert_out, SP, split_axis=0, concat_axis=0, tiled=True)]
    slice x4 -> x0, local copies, waits for them, and re-layouts: 4.1 us -> none  [the longest x1 1.2 us: local(): flat[:, DK_A:]]
  transfers between devices with their start and end apart: 3 -> 0, of which waited for: 3 -> 0; matrix products, arithmetic and copies ran while one was open for 0% -> 0% of each run, Pallas kernels for 0% -> 0%
where the time goes in v2:
time: 137 us; the launch traced here: 135 us
  Pallas kernels  125 us (91%)
  other arithmetic  6.51 us (5%)
  local copies, waits for them, and re-layouts  3.65 us (3%)
    pallas_call x1, Pallas kernels, layer(): pl.pallas_call(functools.partial(layer_kernel, scale_one=scale_one, scale...  125 us

profile of v2, /device:TPU:2, one launch (start us, length us, event | category | flops | bytes accessed | tf_op | source)
XLA Modules:
  0.0 135.4 jit_solution(13854644233901193790)
XLA Ops:
  0.0 0.0 copy-start
  0.0 0.0 copy-start.1
  0.0 0.0 copy-start.2
  0.0 0.8 convert.17
  0.9 0.7 convert_element_type.32
  1.6 0.2 subtract_convert_fusion.1
  1.8 0.8 copy.39.turned_ref
  2.6 1.2 fusion.1
  3.8 1.2 fusion.3
  4.9 0.8 fusion.4.own_ref
  5.7 0.0 copy-done
  5.7 0.1 constant_dynamic-slice_fusion
  5.8 0.1 copy.40
  5.9 0.1 eq.17
  6.0 0.2 convert_reduce_fusion
  6.2 0.1 reduce_sum.31
  6.3 0.1 copy.36
  6.4 0.7 tile.10.slots_ref
  7.1 0.1 add.86
  7.1 0.1 add.87
  7.2 0.7 bitcast_add_fusion.spots_ref
  7.9 0.0 copy-done.1
  7.9 0.0 copy-done.2
  7.9 0.1 copy.37
  8.0 0.7 broadcast_divide_fusion.share_ref
  8.7 125.1 %layer.1 = bf16[24,2048]{1,0:T(8,128)(2,1)} custom-call(bf16[384,256]{1,0:T(8,128)(2,1)} %bitcast.18, bf16[384,64]{1,0:T(8,128)(2,1)} %copy.39.turned_ref, bf16[416,512]{1,0:T(8,128)(2,1)} %fusion.4.own_ref, bf16[512,256]{1,0:T(8,128)(2,1)} %bitcast.15, bf16[512,256]{1,0:T(8,128)(2,1)} %bitcast.16, bf16[256,2048]{1,0:T(8,128)(2,1)} %bitcast.14, ...), custom_call_target="tpu_custom_call" | custom-call | tf_op jit(solution)/shard_map/layer/pallas_call | solution.py:560
  133.8 1.5 %copy.42 = bf16[24,2048]{1,0:T(8,128)(2,1)} copy(bf16[24,2048]{1,0:T(8,128)(2,1)} %layer.1) | data formatting | bytes 196608
  (10 shorter events, 0.1 us)
Async XLA Ops:
  0.0 5.7 %copy-start = (s32[384,2]{0,1:T(2,128)S(1)}, s32[384,2]{0,1:T(2,128)}, u32[]{:S(2)}) copy-start(s32[384,2]{0,1:T(2,128)} %param.26) | copy-start | bytes 9220
  0.0 7.9 %copy-start.1 = (f32[24,2]{0,1:T(2,128)S(1)}, f32[24,2]{0,1:T(2,128)}, u32[]{:S(2)}) copy-start(f32[24,2]{0,1:T(2,128)} %param.28) | copy-start | bytes 580
  0.0 7.9 %copy-start.2 = (f32[24]{0:T(128)S(1)}, f32[24]{0:T(128)}, u32[]{:S(2)}) copy-start(f32[24]{0:T(128)} %param.27) | copy-start | bytes 292

commit v3 on v2

--- a/solution.py
+++ b/solution.py
@@ -2,6 +2,7 @@
 
 import jax
 import jax.numpy as jnp
+import numpy as np
 from jax import lax
 from jax.experimental import pallas as pl
 from jax.experimental.pallas import tpu as pltpu
@@ -59,10 +60,11 @@
 
 
 def layer_kernel(
-    q_ref, turned_ref, own_ref, wk_ref, wv_ref, ow_ref, residual_ref, gain_ref,
-    slots_ref, spots_ref, share_ref, gate_hbm, up_hbm, down_hbm, out_ref,
-    qx, wkt, wvx, buf, kta, ktb, vx, acc, top, owp, attx, attr, part,
-    far_out, far_in, step_out, step_in, mixed_ref, disp, arr, rows_ref,
+    q_ref, q_rope_ref, latent_ref, key_rope_ref, latent_gain_ref, pace_ref,
+    wk_ref, wv_ref, ow_ref, residual_ref, gain_ref,
+    routes_ref, group_ref, share_ref, gate_hbm, up_hbm, down_hbm, out_ref,
+    own_ref, sel, qx, wkt, buf, kta, ktb, vx, acc, top, weight_sum, owp, attx, attr, part,
+    step_out, step_in, mixed_ref, disp, arr, rows_ref,
     held, gate, up, down, made, given, rs_out, rs_in, sums_ref, ret, back,
     ring_send, ring_recv, flip_send, flip_recv, misc_send, misc_recv, head_send, head_recv,
     disp_send, disp_recv, load_sem, z_send, z_recv, swap_send, swap_recv,
@@ -97,6 +99,21 @@
     ]
     for load in loads:
         load.start()
+    angles = (me * 384 + lax.broadcasted_iota(jnp.int32, (16, 384), 1)).astype(F32)
+    angles = angles * pace_ref[...]
+    cosine = jnp.cos(angles)
+    sine = jnp.sin(angles)
+
+    def turn(pair):
+        first, second = pair[0:16], pair[16:32]
+        return [first * cosine - second * sine, second * cosine + first * sine]
+
+    keys = key_rope_ref[...].astype(F32)
+    own_ref[0:32, 0:384] = jnp.concatenate(turn(keys), axis=0).astype(BF)
+    own_ref[0:32, 384:512] = jnp.zeros((32, 128), BF)
+    latent = latent_ref[...].astype(F32)
+    inverse = lax.rsqrt(jnp.mean(latent * latent, axis=1, keepdims=True) + epsilon)
+    own_ref[32:416] = (latent * inverse * latent_gain_ref[...]).astype(BF)
     meet([partner, along_z(1), along_z(-1)] + [peer[2] for peer in peers])
     start_row = c * HALF
     other_row = (1 - c) * HALF
@@ -158,13 +175,14 @@
 
     for sign in (1, -1):
         send(None, slot(-sign, 0), along_a(sign))
-        send(None, slot(0, -sign), along_b(sign))
     weights_over = pltpu.make_async_remote_copy(
         src_ref=ow_ref, dst_ref=owp, send_sem=misc_send.at[0], recv_sem=misc_recv.at[0],
         device_id=partner, device_id_type=MESH,
     )
     weights_over.start()
 
+    queries = q_rope_ref[...].astype(F32)
+    turned = jnp.concatenate(turn(queries[0:32]) + turn(queries[32:64]), axis=0).astype(BF)
     spread = chosen(
         lax.broadcasted_iota(jnp.int32, (256, 384), 1)
         == spread_place(lax.broadcasted_iota(jnp.int32, (256, 384), 0))
@@ -176,9 +194,10 @@
     )
     qx[...] = (
         jnp.dot(q_ref[...], spread, preferred_element_type=F32)
-        + jnp.dot(turned_ref[...], turns, preferred_element_type=F32)
+        + lax.dot_general(
+            turned, turns, (((0,), (0,)), ((), ())), preferred_element_type=F32
+        )
     ).astype(BF)
-    wvx[...] = jnp.dot(wv_ref[...], spread, preferred_element_type=F32).astype(BF)
     unit = chosen(
         lax.broadcasted_iota(jnp.int32, (256, 256), 0)
         == lax.broadcasted_iota(jnp.int32, (256, 256), 1)
@@ -186,10 +205,27 @@
     wkt[...] = lax.dot_general(
         unit, wk_ref[...], (((1,), (1,)), ((), ())), preferred_element_type=F32
     ).astype(BF)
+    tokens = lax.broadcasted_iota(jnp.int32, (24, 384), 0) + (z * 2 + c) * 24
+    mine = chosen(lax.broadcasted_iota(jnp.int32, (24, 384), 1) == tokens)
+    routes = lax.dot_general(
+        mine, routes_ref[...].astype(F32).astype(BF), (((1,), (1,)), ((), ())),
+        preferred_element_type=F32,
+    )
+    experts = lax.broadcasted_iota(jnp.int32, (24, 32), 1).astype(F32)
+    named = [routes[:, k : k + 1] == experts for k in (0, 1)]
+    earlier = chosen(
+        lax.broadcasted_iota(jnp.int32, (24, 24), 0) > lax.broadcasted_iota(jnp.int32, (24, 24), 1)
+    )
+    before = jnp.dot(earlier, chosen(named[0] | named[1]), preferred_element_type=F32)
+    packed = lax.broadcasted_iota(jnp.int32, (96, 256), 1).astype(F32)
+    for k in (0, 1):
+        rank = jnp.sum(jnp.where(named[k], before, 0.0), axis=1, keepdims=True)
+        expert = routes[:, k : k + 1]
+        spot = jnp.floor(expert * 0.5) * 12.0 + expert * 2.0 + rank
+        spots = jnp.concatenate([spot + 4.0 * j for j in range(4)], axis=0)
+        sel[k] = chosen(packed == spots)
     kta[96:128] = jnp.zeros((32, 384), BF)
     ktb[224:256] = jnp.zeros((32, 384), BF)
-    lanes = lax.broadcasted_iota(jnp.int32, (1, 384), 1)
-    ones = jnp.where((lanes == 64) | (lanes == 320), 1.0, 0.0)
     heads = (
         (slice(0, 128), kta, 0, scale_one * LOG2E),
         (slice(128, 384), ktb, 1, scale_two * LOG2E),
@@ -205,7 +241,7 @@
         kta[64:96] = rope
         ktb[0:192] = keys[64:256]
         ktb[192:224] = rope
-        vx[...] = (jnp.dot(lat, wvx[...], preferred_element_type=F32) + ones).astype(BF)
+        vx[...] = jnp.dot(lat, wv_ref[...], preferred_element_type=F32).astype(BF)
         for cols, keys_ref, h, factor in heads:
             scores = jnp.dot(qx[:, cols], keys_ref[...], preferred_element_type=F32)
             if first:
@@ -220,16 +256,19 @@
                 old = top[h]
                 new = jnp.maximum(old, peak)
             top[h] = new
-            weights = jnp.exp2(
-                (scores - jnp.concatenate([new] * 3, axis=1)) * factor
-            ).astype(BF)
-            update = jnp.dot(weights, vx[:, cols], preferred_element_type=F32)
+            weights = jnp.exp2((scores - jnp.concatenate([new] * 3, axis=1)) * factor)
+            sums = weights[:, 0:128] + weights[:, 128:256] + weights[:, 256:384]
+            update = jnp.dot(weights.astype(BF), vx[:, 0 : 128 * width], preferred_element_type=F32)
             if first:
+                weight_sum[h] = sums
                 acc[:, cols] = update
             else:
                 shrink = jnp.exp2((old - new) * factor)
+                weight_sum[h] = weight_sum[h] * shrink + sums
                 acc[:, cols] = acc[:, cols] * jnp.concatenate([shrink] * width, axis=1) + update
 
+    for sign in (1, -1):
+        send(None, slot(0, -sign), along_b(sign))
     block(own_ref, True)
 
     def step(i, carry):
@@ -250,7 +289,7 @@
                 send(k, slot(-sign, -1), along_b(1))
                 send(k, slot(-sign, 1), along_b(-1))
 
-        @pl.when(i == 5)
+        @pl.when(i == 4)
         def _():
             k = slot(2, 0)
             arrived(k, 0)
@@ -272,20 +311,23 @@
                     flip(k)
                     send(k, slot(da, -2 * sign), along_b(sign), 0 if sign == 1 else 1)
 
-        @pl.when(i == 11)
+        @pl.when(i == 8)
         def _():
             for sign in (1, -1):
                 k = slot(2, -sign)
                 arrived(k)
                 flip(k)
                 send(k, slot(2, -2 * sign), along_b(sign), 0 if sign == 1 else 1)
+
+        @pl.when(i == 10)
+        def _():
             for da in (-1, 1):
                 k = slot(da, 2)
                 arrived(k, 0)
                 arrived(k, 1)
                 flip(k)
 
-        @pl.when(i == 15)
+        @pl.when(i == 11)
         def _():
             k = slot(2, 2)
             arrived(k, 0)
@@ -309,9 +351,10 @@
     lax.fori_loop(1, 16, step, 0)
 
     total = acc[...]
-    part_a = total[:, 0:128] / total[:, 64:65]
-    part_b = total[:, 128:384] / total[:, 320:321]
-    both = jnp.concatenate([part_a, part_b], axis=1)
+    part_a = total[:, 0:128] / jnp.sum(weight_sum[0], axis=1, keepdims=True)
+    part_b = total[:, 128:384] / jnp.sum(weight_sum[1], axis=1, keepdims=True)
+    low = lax.broadcasted_iota(jnp.int32, (384, 128), 1) < DV_A
+    both = jnp.concatenate([jnp.where(low, part_a, part_b[:, 0:128]), part_b[:, 128:256]], axis=1)
     for side in (0, 1):
         attx[side] = jnp.concatenate(
             [both[(2 * k + side) * 24 : (2 * k + side + 1) * 24] for k in range(8)], axis=0
@@ -322,61 +365,61 @@
     )
     heads_over.start()
     weights_over.wait_recv()
-    mine = attx[c]
-    partial = jnp.dot(mine[:, 0:64], ow_ref[0:64], preferred_element_type=F32)
-    partial = partial + jnp.dot(mine[:, 128:320], ow_ref[64:256], preferred_element_type=F32)
+    partial = jnp.dot(attx[c], ow_ref[...], preferred_element_type=F32)
     heads_over.wait_recv()
-    theirs = attr[...]
-    partial = partial + jnp.dot(theirs[:, 0:64], owp[0:64], preferred_element_type=F32)
-    partial = partial + jnp.dot(theirs[:, 128:320], owp[64:256], preferred_element_type=F32)
+    partial = partial + jnp.dot(attr[...], owp[...], preferred_element_type=F32)
     part[...] = partial.reshape(8, 24, 2048)
 
     sent = []
-
-    def pass_on(src, dst, sign, k):
-        way = 0 if sign == 1 else 1
+    chains = {}
+
+    def pass_on(way, side, hop, value):
+        step_out[way, side, hop] = value.astype(BF)
         copy = pltpu.make_async_remote_copy(
-            src_ref=src, dst_ref=dst, send_sem=head_send.at[way, k], recv_sem=head_recv.at[way, k],
-            device_id=along_z(sign), device_id_type=MESH,
+            src_ref=step_out.at[way, side, hop], dst_ref=step_in.at[way, side, hop],
+            send_sem=head_send.at[way, side, hop], recv_sem=head_recv.at[way, side, hop],
+            device_id=along_z(1 if way == 0 else -1), device_id_type=MESH,
         )
         copy.start()
         sent.append(copy)
-        return copy
-
-    ways = ((1, 0, slice(0, 1024)), (-1, 1, slice(1024, 2048)))
-    pending = {}
-    for sign, way, cols in ways:
-        far_out[way] = part[(z + 4) % 8, :, cols].astype(BF)
-        pending[sign] = pass_on(far_out.at[way], far_in.at[way], sign, 0)
+        chains[way, side] = copy
+
+    def head_part(dz, side):
+        return part[(z + dz + 8) % 8, :, side * 512 : (side + 1) * 512]
+
+    far = ((0, 0), (1, 2), (0, 1), (1, 3))
+    near = ((0, 2), (1, 0), (0, 3), (1, 1))
+    for way, side in far:
+        pass_on(way, side, 0, head_part(4, side))
+    for way, side in near:
+        pass_on(way, side, 1, head_part(3 if way == 0 else -3, side))
     for hop in (1, 2, 3):
-        for sign, way, cols in ways:
-            pending[sign].wait_recv()
-            mine = part.at[(z + sign * (4 - hop) + 8) % 8]
-            if hop == 1:
-                inside = mine[:, cols] + far_in[way].astype(F32)
-                outside = mine[:, 1024:2048] if way == 0 else mine[:, 0:1024]
-                pair = [inside, outside] if way == 0 else [outside, inside]
-                value = jnp.concatenate(pair, axis=1)
-            else:
-                value = mine[...] + step_in[way, hop - 2].astype(F32)
-            step_out[way, hop - 1] = value.astype(BF)
-            pending[sign] = pass_on(
-                step_out.at[way, hop - 1], step_in.at[way, hop - 1], sign, hop
-            )
-    pending[1].wait_recv()
-    pending[-1].wait_recv()
+        for way, side in far:
+            chains[way, side].wait_recv()
+            dz = (4 - hop) * (1 if way == 0 else -1)
+            got = step_in[way, side, hop - 1].astype(F32)
+            pass_on(way, side, hop, head_part(dz, side) + got)
+        if hop < 3:
+            for way, side in near:
+                chains[way, side].wait_recv()
+                dz = (3 - hop) * (1 if way == 0 else -1)
+                got = step_in[way, side, hop].astype(F32)
+                pass_on(way, side, hop + 1, head_part(dz, side) + got)
+    for chain in chains.values():
+        chain.wait_recv()
+    arrived_sums = [
+        jnp.concatenate([step_in[way, side, 3] for side in range(4)], axis=1).astype(F32)
+        for way in (0, 1)
+    ]
     mixed = residual_ref[...].astype(F32) + part[z]
-    mixed = mixed + step_in[0, 2].astype(F32) + step_in[1, 2].astype(F32)
+    mixed = mixed + arrived_sums[0] + arrived_sums[1]
     mixed_ref[...] = mixed
     inverse = lax.rsqrt(jnp.mean(mixed * mixed, axis=1, keepdims=True) + epsilon)
     normed = mixed * inverse * gain_ref[...]
     stack = jnp.concatenate([normed[:, j * 512 : (j + 1) * 512] for j in range(4)], axis=0)
-    rows = lax.broadcasted_iota(jnp.int32, (256, 96), 0)
-    columns = lax.broadcasted_iota(jnp.int32, (256, 96), 1)
-    wanted = (rows // 16) * 4 + rows % 4
-    hit = (wanted == slots_ref[0:1, :]) | (wanted == slots_ref[1:2, :])
-    pick = chosen(hit & ((rows // 4) % 4 == columns // 24))
-    outgoing = jnp.dot(pick, stack.astype(BF), preferred_element_type=F32).astype(BF)
+    outgoing = lax.dot_general(
+        sel[0] + sel[1], stack.astype(BF), (((0,), (0,)), ((), ())), preferred_element_type=F32
+    ).astype(BF)
     disp[...] = outgoing.reshape(16, 16, 512)
 
     def exchange(source, target, send_sem, recv_sem):
@@ -533,13 +576,17 @@
     moves += exchange(ret, back, back_send, back_recv)
     returned = back[...].reshape(256, 512)
     result = mixed_ref[...]
-    spots = lax.broadcasted_iota(jnp.int32, (96, 256), 1)
+    eye = lax.broadcasted_iota(jnp.int32, (24, 24), 0)
+    eye = eye == lax.broadcasted_iota(jnp.int32, (24, 24), 1)
+    groups = jnp.sum(jnp.where(eye, group_ref[...], 0.0), axis=1, keepdims=True)
+    shares = [
+        jnp.sum(jnp.where(eye, share_ref[k : k + 1], 0.0), axis=1, keepdims=True) for k in (0, 1)
+    ]
     for k in (0, 1):
-        select = chosen(spots == spots_ref[:, k : k + 1])
-        picked = jnp.dot(select, returned, preferred_element_type=F32)
+        picked = jnp.dot(sel[k], returned, preferred_element_type=F32)
         picked = jnp.concatenate([picked[j * 24 : (j + 1) * 24] for j in range(4)], axis=1)
-        result = result + share_ref[:, k : k + 1] * picked
-    out_ref[...] = result.astype(BF)
+        result = result + groups * shares[k] / (shares[0] + shares[1]) * picked
+    out_ref[...] = result
     for copy in copies + moves:
         copy.wait_send()
     ends = [(ring_send.at[k], size) for k, size in ring]
@@ -559,27 +606,27 @@
     dma = pltpu.SemaphoreType.DMA
     return pl.pallas_call(
         functools.partial(layer_kernel, scale_one=scale_one, scale_two=scale_two),
-        out_shape=jax.ShapeDtypeStruct((24, 2048), BF),
+        out_shape=jax.ShapeDtypeStruct((24, 2048), F32),
         in_specs=[vmem] * len(operands) + [hbm] * len(weights),
         out_specs=vmem,
         scratch_shapes=[
+            pltpu.VMEM((416, 512), BF),
+            pltpu.VMEM((2, 96, 256), BF),
             pltpu.VMEM((384, 384), BF),
             pltpu.VMEM((256, 512), BF),
-            pltpu.VMEM((512, 384), BF),
             pltpu.VMEM((15, 416, 512), BF),
             pltpu.VMEM((128, 384), BF),
             pltpu.VMEM((256, 384), BF),
-            pltpu.VMEM((384, 384), BF),
+            pltpu.VMEM((384, 256), BF),
             pltpu.VMEM((384, 384), F32),
             pltpu.VMEM((2, 384, 128), F32),
+            pltpu.VMEM((2, 384, 128), F32),
             pltpu.VMEM((256, 2048), BF),
-            pltpu.VMEM((2, 192, 384), BF),
-            pltpu.VMEM((192, 384), BF),
+            pltpu.VMEM((2, 192, 256), BF),
+            pltpu.VMEM((192, 256), BF),
             pltpu.VMEM((8, 24, 2048), F32),
-            pltpu.VMEM((2, 24, 1024), BF),
-            pltpu.VMEM((2, 24, 1024), BF),
-            pltpu.VMEM((2, 3, 24, 2048), BF),
-            pltpu.VMEM((2, 3, 24, 2048), BF),
+            pltpu.VMEM((2, 4, 4, 24, 512), BF),
+            pltpu.VMEM((2, 4, 4, 24, 512), BF),
             pltpu.VMEM((24, 2048), F32),
             pltpu.VMEM((16, 16, 512), BF),
             pltpu.VMEM((16, 16, 512), BF),
@@ -601,8 +648,8 @@
             dma((15,)),
             dma((2,)),
             dma((2,)),
-            dma((2, 4)),
-            dma((2, 4)),
+            dma((2, 4, 4)),
+            dma((2, 4, 4)),
             dma((15,)),
             dma((15,)),
             dma((3,)),
@@ -624,28 +671,6 @@
     )(*operands, *weights)
 
 
-def angle_tables(places, rope_width):
-    frequencies = rope_base ** (-jnp.arange(0, rope_width, 2, dtype=jnp.float32) / rope_width)
-    angles = places[:, None] * frequencies[None, :]
-    return (jnp.cos(angles), jnp.sin(angles))
-
-
-def rope_turn(values, cosine, sine_table):
-    half_size = values.shape[-1] // 2
-    first_half = values[..., :half_size]
-    second = values[..., half_size:]
-    return jnp.concatenate(
-        [first_half * cosine - second * sine_table, second * cosine + first_half * sine_table],
-        axis=-1,
-    )
-
-
-def rms_scale(values, gain_vector):
-    values = values.astype(jnp.float32)
-    inverse = lax.rsqrt(jnp.mean(values * values, axis=-1, keepdims=True) + epsilon)
-    return values * inverse * gain_vector
-
-
 def local(
     residual,
     queries,
@@ -664,50 +689,28 @@
     up_weight,
     down_weight,
 ):
-    local_tokens = queries.shape[0]
-    pair_dev = queries.shape[1]
-    tp_count = lax.axis_size(TP)
-    row_count = local_tokens // tp_count
     rope_width = key_rope.shape[1]
-    first_place = lax.axis_index(SP) * local_tokens
-    places = (first_place + jnp.arange(local_tokens, dtype=jnp.int32)).astype(jnp.float32)
-    cosine, sine_table = angle_tables(places, rope_width)
-    rotated_key = rope_turn(key_rope.astype(jnp.float32), cosine, sine_table).astype(jnp.bfloat16)
-    turned = rope_turn(
-        query_rope.astype(jnp.float32).reshape(local_tokens, pair_dev, 2, rope_width),
-        cosine[:, None, None, :],
-        sine_table[:, None, None, :],
-    ).astype(jnp.bfloat16)
-    compressed = rms_scale(latent, latent_gain).astype(BF)
     scale_one = (DK_A + rope_width) ** (-0.5)
     scale_two = (queries.shape[2] - DK_A + rope_width) ** (-0.5)
-    own = jnp.concatenate(
-        [jnp.pad(rotated_key.T, ((0, 0), (0, 128))), compressed], axis=0
-    )
-    flat = queries[:, 0]
-    own_routes = lax.dynamic_slice_in_dim(routes, lax.axis_index(TP) * row_count, row_count, 0)
-    choices = own_routes.reshape(-1)
-    order = jnp.arange(choices.shape[0], dtype=jnp.int32)
-    same = (choices[:, None] == choices[None, :]) & (order[:, None] > order[None, :])
-    slots = (choices * 2 + jnp.sum(same.astype(jnp.int32), axis=1)).reshape(row_count, 2)
-    spots = (slots // 4) * 16 + slots % 4
-    quarters = jnp.arange(4, dtype=jnp.int32)
-    spots = (spots[None] + 4 * quarters[:, None, None]).reshape(4 * row_count, 2)
-    route_weight = group_gate[:, None] * expert_share / jnp.sum(expert_share, axis=1, keepdims=True)
+    pace = np.float64(rope_base) ** (-np.arange(0, rope_width, 2) / rope_width)
     operands = (
-        flat,
-        turned.reshape(local_tokens, 2 * rope_width),
-        own,
+        queries[:, 0],
+        query_rope[:, 0].T,
+        latent,
+        key_rope.T,
+        latent_gain[None],
+        jnp.asarray(pace[:, None], F32),
         key_weight[:, 0],
         value_weight[:, 0],
         out_weight[0],
         residual,
         norm_gain[None],
-        jnp.tile(slots.T, (1, 4)),
-        spots,
-        route_weight,
-    )
-    return layer(operands, (gate_weight, up_weight, down_weight), scale_one, scale_two)
+        routes.T,
+        group_gate[None],
+        expert_share.T,
+    )
+    out = layer(operands, (gate_weight, up_weight, down_weight), scale_one, scale_two)
+    return out.astype(BF)
 
 
 def solution(mesh):

time: 137 us -> 122 us (0.89)
  Pallas kernels: 125 us -> 120 us
  other arithmetic: 6.51 us -> 1.58 us
  local copies, waits for them, and re-layouts: 3.65 us -> 0 us
    pallas_call x1, Pallas kernels: 125 us -> 120 us  [layer(): pl.pallas_call(functools.partial(layer_kernel, scale_one=scale_one, scale...]
    unnamed x8 -> x0, local copies, waits for them, and re-layouts: 1.64 us -> none
where the time goes in v3:
time: 122 us; the launch traced here: 121 us
  Pallas kernels  120 us (98%)
  other arithmetic  1.58 us (1%)
    pallas_call x1, Pallas kernels, layer(): pl.pallas_call(functools.partial(layer_kernel, scale_one=scale_one, scale...  120 us

profile of v3, /device:TPU:2, one launch (start us, length us, event | category | flops | bytes accessed | tf_op | source)
XLA Modules:
  0.0 121.1 jit_solution(849118240889369581)
XLA Ops:
  0.0 119.5 %layer.1 = f32[24,2048]{1,0:T(8,128)} custom-call(bf16[384,256]{1,0:T(8,128)(2,1)} %bitcast.16, bf16[64,384]{1,0:T(8,128)(2,1)} %bitcast.17, bf16[384,512]{1,0:T(8,128)(2,1)} %latent_ref.1, bf16[32,384]{1,0:T(8,128)(2,1)} %bitcast.18, f32[1,512]{1,0:T(1,128)} %bitcast.21, f32[16,1]{1,0:T(8,128)} %constant.2.clone.pace_ref, bf16[512,256]{1,0:T(8,128)(2,1)} %bitcast.14, ...), custom_call_target="tpu_custom_call" | custom-call | tf_op jit(solution)/shard_map/layer/pallas_call | solution.py:607
  119.5 1.6 %convert_element_type.3 = bf16[24,2048]{1,0:T(8,128)(2,1)} convert(f32[24,2048]{1,0:T(8,128)} %layer.1) | non-fusion elementwise | flops 49152 | bytes 294912 | tf_op jit(solution)/shard_map/convert_element_type | solution.py:713

commit v4 on v3

--- a/solution.py
+++ b/solution.py
@@ -91,7 +91,7 @@
     me = y * 4 + x
     peers = [
         (dy, dx, ((y + dy) % 4, (x + dx) % 4, z, c))
-        for dy in range(4) for dx in range(4) if dy or dx
+        for dy, dx in sorted(ORDER[1:], key=lambda p: -(min(p[0], 4 - p[0]) + min(p[1], 4 - p[1])))
     ]
     loads = [
         pltpu.make_async_copy(src, dst, load_sem.at[k])
@@ -289,7 +289,7 @@
                 send(k, slot(-sign, -1), along_b(1))
                 send(k, slot(-sign, 1), along_b(-1))
 
-        @pl.when(i == 4)
+        @pl.when(i == 3)
         def _():
             k = slot(2, 0)
             arrived(k, 0)
@@ -302,7 +302,7 @@
             arrived(k, 1)
             flip(k)
 
-        @pl.when(i == 7)
+        @pl.when(i == 6)
         def _():
             for da in (-1, 1):
                 for sign in (1, -1):
@@ -311,7 +311,7 @@
                     flip(k)
                     send(k, slot(da, -2 * sign), along_b(sign), 0 if sign == 1 else 1)
 
-        @pl.when(i == 8)
+        @pl.when(i == 7)
         def _():
             for sign in (1, -1):
                 k = slot(2, -sign)
@@ -319,7 +319,7 @@
                 flip(k)
                 send(k, slot(2, -2 * sign), along_b(sign), 0 if sign == 1 else 1)
 
-        @pl.when(i == 10)
+        @pl.when(i == 9)
         def _():
             for da in (-1, 1):
                 k = slot(da, 2)
@@ -327,7 +327,7 @@
                 arrived(k, 1)
                 flip(k)
 
-        @pl.when(i == 11)
+        @pl.when(i == 10)
         def _():
             k = slot(2, 2)
             arrived(k, 0)
@@ -462,108 +462,135 @@
         return copy
 
     hops = {}
-    flips = {}
-    for e in (0, 1):
-        for way, sign in ((0, 1), (1, -1)):
+    swaps = {}
+    ways = ((0, 1), (1, -1))
+
+    def expert_of(way, unit):
+        return unit if way == 0 else 1 - unit
+
+    for unit in (0, 1):
+        for way, sign in ways:
+            e = expert_of(way, unit)
             hops[way, 1, e] = remote(
                 rows_ref.at[e], held.at[e, BASE[-sign] + c],
                 z_send.at[way, 0, e], z_recv.at[way, 0, e], along_z(sign),
             )
-        flips[0, e] = remote(
+    for e in (0, 1):
+        swaps[0, e] = remote(
             rows_ref.at[e], held.at[e, c], swap_send.at[0, e], swap_recv.at[0, e], partner
         )
         held[e, c] = rows_ref[e]
 
-    def compute(first, count, dzs):
-        for e in (0, 1):
-            rows = held[e, first : first + count].reshape(count * 32, 2048)
-            inner = jnp.dot(rows, gate[e], preferred_element_type=F32)
-            inner = inner / (1.0 + jnp.exp(-inner))
-            inner = inner * jnp.dot(rows, up[e], preferred_element_type=F32)
-            result = jnp.dot(inner.astype(BF), down[e], preferred_element_type=F32)
-            made[e, first : first + count] = result.astype(BF).reshape(count, 32, 2048)
-            for dz in dzs:
-                k = BASE[dz] // 2
-                gives[dz, e] = remote(
-                    made.at[e, BASE[dz] + 1 - c], given.at[e, k],
-                    give_send.at[k, e], give_recv.at[k, e], partner,
+    def compute(e, dz):
+        first = BASE[dz]
+        k = first // 2
+        swaps[k, e].wait_recv()
+        rows = held[e, first : first + 2].reshape(64, 2048)
+        inner = jnp.dot(rows, gate[e], preferred_element_type=F32)
+        inner = inner / (1.0 + jnp.exp(-inner))
+        inner = inner * jnp.dot(rows, up[e], preferred_element_type=F32)
+        result = jnp.dot(inner.astype(BF), down[e], preferred_element_type=F32)
+        made[e, first : first + 2] = result.astype(BF).reshape(2, 32, 2048)
+        gives[dz, e] = remote(
+            made.at[e, first + 1 - c], given.at[e, k], give_send.at[k, e], give_recv.at[k, e],
+            partner,
+        )
+
+    def relay(dist, unit):
+        for way, sign in ways:
+            e = expert_of(way, unit)
+            hops[way, dist, e].wait_recv()
+            dz = -sign * dist
+            spot = held.at[e, BASE[dz] + c]
+            k = BASE[dz] // 2
+            target = None
+            if dist < 3:
+                target = held.at[e, BASE[dz - sign] + c]
+            elif unit == 0:
+                target = held.at[e, BASE[4] + c]
+            if target is not None:
+                hops[way, dist + 1, e] = remote(
+                    spot, target, z_send.at[way, dist, e], z_recv.at[way, dist, e], along_z(sign)
                 )
+            swaps[k, e] = remote(spot, spot, swap_send.at[k, e], swap_recv.at[k, e], partner)
+
+    def work(dist, unit):
+        for way, sign in ways:
+            compute(expert_of(way, unit), -sign * dist)
 
     gives = {}
 
-    def chip_sum(dz, e):
+    def chip_sum(dz, e, side):
         if (dz, e) in gives:
             gives.pop((dz, e)).wait_recv()
-        return made[e, BASE[dz] + c].astype(F32) + given[e, BASE[dz] // 2].astype(F32)
+        rows = slice(side * 16, (side + 1) * 16)
+        mine = made[e, BASE[dz] + c, rows].astype(F32)
+        return mine + given[e, BASE[dz] // 2, rows].astype(F32)
 
     for load in loads:
         load.wait()
     for e in (0, 1):
-        flips[0, e].wait_recv()
-    compute(0, 2, (0,))
-    for dist in (1, 2, 3):
-        for e in (0, 1):
-            for way, sign in ((0, 1), (1, -1)):
-                hops[way, dist, e].wait_recv()
-                dz = -sign * dist
-                spot = held.at[e, BASE[dz] + c]
-                k = BASE[dz] // 2
-                if dist < 3:
-                    target = held.at[e, BASE[dz - sign] + c]
-                elif way == e:
-                    target = held.at[e, BASE[4] + c]
-                else:
-                    target = None
-                if target is not None:
-                    hops[way, dist + 1, e] = remote(
-                        spot, target, z_send.at[way, dist, e], z_recv.at[way, dist, e],
-                        along_z(sign),
-                    )
-                flips[k, e] = remote(
-                    spot, spot, swap_send.at[k, e], swap_recv.at[k, e], partner
-                )
-        for e in (0, 1):
-            for dz in (-dist, dist):
-                flips[BASE[dz] // 2, e].wait_recv()
-        compute(4 * dist - 2, 4, (-dist, dist))
+        compute(e, 0)
+    relay(1, 0)
+    relay(1, 1)
+    work(1, 0)
+    relay(2, 0)
+    work(1, 1)
+    relay(2, 1)
+    work(2, 0)
+    relay(3, 0)
+    work(2, 1)
+    work(3, 0)
+    relay(3, 1)
 
     sums = {}
 
-    def push(way, e, hop, value):
-        sign = 1 if way == 0 else -1
-        rs_out[way, e, hop] = value.astype(BF)
-        sums[way, e] = remote(
-            rs_out.at[way, e, hop], rs_in.at[way, e, hop],
-            rs_send.at[way, e, hop], rs_recv.at[way, e, hop], along_z(sign),
+    def push(way, e, side, hop, value):
+        rs_out[way, e, side, hop] = value.astype(BF)
+        sums[way, e, side] = remote(
+            rs_out.at[way, e, side, hop], rs_in.at[way, e, side, hop],
+            rs_send.at[way, e, side, hop], rs_recv.at[way, e, side, hop],
+            along_z(1 if way == 0 else -1),
         )
 
-    push(0, 1, 1, chip_sum(3, 1))
-    push(1, 0, 1, chip_sum(-3, 0))
+    def carry_on(way, e, dz, hop, sides=(0, 1)):
+        for side in sides:
+            sums[way, e, side].wait_recv()
+            got = rs_in[way, e, side, hop - 1].astype(F32)
+            push(way, e, side, hop, chip_sum(dz, e, side) + got)
+
+    for way, e, dz in ((0, 1, 3), (1, 0, -3)):
+        for side in (0, 1):
+            push(way, e, side, 1, chip_sum(dz, e, side))
+    work(3, 1)
     for e in (0, 1):
         hops[e, 4, e].wait_recv()
         spot = held.at[e, BASE[4] + c]
-        flips[7, e] = remote(spot, spot, swap_send.at[7, e], swap_recv.at[7, e], partner)
+        swaps[7, e] = remote(spot, spot, swap_send.at[7, e], swap_recv.at[7, e], partner)
     for e in (0, 1):
-        flips[7, e].wait_recv()
-    compute(14, 2, (4,))
-    push(0, 0, 0, chip_sum(4, 0))
-    push(1, 1, 0, chip_sum(4, 1))
-    for hop in (1, 2, 3):
-        if hop < 3:
-            for way, e in ((0, 1), (1, 0)):
-                sums[way, e].wait_recv()
-                dz = (3 - hop) * (1 if way == 0 else -1)
-                push(way, e, hop + 1, chip_sum(dz, e) + rs_in[way, e, hop].astype(F32))
-        for way, e in ((0, 0), (1, 1)):
-            sums[way, e].wait_recv()
-            dz = (4 - hop) * (1 if way == 0 else -1)
-            push(way, e, hop, chip_sum(dz, e) + rs_in[way, e, hop - 1].astype(F32))
+        compute(e, 4)
+    carry_on(0, 1, 2, 2, (0,))
+    carry_on(1, 0, -2, 2, (0,))
+    for way, e in ((0, 0), (1, 1)):
+        for side in (0, 1):
+            push(way, e, side, 0, chip_sum(4, e, side))
+    carry_on(0, 1, 2, 2, (1,))
+    carry_on(1, 0, -2, 2, (1,))
+    carry_on(0, 0, 3, 1)
+    carry_on(1, 1, -3, 1)
+    carry_on(0, 1, 1, 3)
+    carry_on(1, 0, -1, 3)
+    carry_on(0, 0, 2, 2)
+    carry_on(1, 1, -2, 2)
+    carry_on(0, 0, 1, 3)
+    carry_on(1, 1, -1, 3)
     for e in (0, 1):
-        own = chip_sum(0, e)
-        for way in (0, 1):
-            sums[way, e].wait_recv()
-            own = own + rs_in[way, e, 3].astype(F32)
-        sums_ref[e] = own.astype(BF)
+        for side in (0, 1):
+            own = chip_sum(0, e, side)
+            for way in (0, 1):
+                sums[way, e, side].wait_recv()
+                own = own + rs_in[way, e, side, 3].astype(F32)
+            sums_ref[e, side * 16 : (side + 1) * 16] = own.astype(BF)
     collected = jnp.concatenate(
         [sums_ref[:, :, j * 512 : (j + 1) * 512].reshape(64, 512) for j in range(4)], axis=0
     )
@@ -637,8 +664,8 @@
             pltpu.VMEM((2, 256, 2048), BF),
             pltpu.VMEM((2, 16, 32, 2048), BF),
             pltpu.VMEM((2, 8, 32, 2048), BF),
-            pltpu.VMEM((2, 2, 4, 32, 2048), BF),
-            pltpu.VMEM((2, 2, 4, 32, 2048), BF),
+            pltpu.VMEM((2, 2, 2, 4, 16, 2048), BF),
+            pltpu.VMEM((2, 2, 2, 4, 16, 2048), BF),
             pltpu.VMEM((2, 32, 2048), BF),
             pltpu.VMEM((16, 16, 512), BF),
             pltpu.VMEM((16, 16, 512), BF),
@@ -659,8 +686,8 @@
             dma((8, 2)),
             dma((8, 2)),
             dma((8, 2)),
-            dma((2, 2, 4)),
-            dma((2, 2, 4)),
+            dma((2, 2, 2, 4)),
+            dma((2, 2, 2, 4)),
             dma((15,)),
             dma((15,)),
         ],

time: 122 us -> 119 us (0.975)
  Pallas kernels: 120 us -> 118 us
    pallas_call x1, Pallas kernels: 120 us -> 118 us  [layer(): pl.pallas_call(functools.partial(layer_kernel, scale_one=scale_one, scale...]
where the time goes in v4:
time: 119 us
  Pallas kernels  118 us (99%)
  other arithmetic  1.58 us (1%)
    pallas_call x1, Pallas kernels, layer(): pl.pallas_call(functools.partial(layer_kernel, scale_one=scale_one, scale...  118 us

profile of v4, /device:TPU:2, one launch (start us, length us, event | category | flops | bytes accessed | tf_op | source)
XLA Modules:
  0.0 119.2 jit_solution(17169213208144521017)
XLA Ops:
  0.0 117.6 %layer.1 = f32[24,2048]{1,0:T(8,128)} custom-call(bf16[384,256]{1,0:T(8,128)(2,1)} %bitcast.16, bf16[64,384]{1,0:T(8,128)(2,1)} %bitcast.17, bf16[384,512]{1,0:T(8,128)(2,1)} %latent_ref.1, bf16[32,384]{1,0:T(8,128)(2,1)} %bitcast.18, f32[1,512]{1,0:T(1,128)} %bitcast.21, f32[16,1]{1,0:T(8,128)} %constant.2.clone.pace_ref, bf16[512,256]{1,0:T(8,128)(2,1)} %bitcast.14, ...), custom_call_target="tpu_custom_call" | custom-call | tf_op jit(solution)/shard_map/layer/pallas_call | solution.py:634
  117.6 1.6 %convert_element_type.3 = bf16[24,2048]{1,0:T(8,128)(2,1)} convert(f32[24,2048]{1,0:T(8,128)} %layer.1) | non-fusion elementwise | flops 49152 | bytes 294912 | tf_op jit(solution)/shard_map/convert_element_type | solution.py:740

commit v5 on v4

--- a/solution.py
+++ b/solution.py
@@ -242,8 +242,11 @@
         ktb[0:192] = keys[64:256]
         ktb[192:224] = rope
         vx[...] = jnp.dot(lat, wv_ref[...], preferred_element_type=F32).astype(BF)
-        for cols, keys_ref, h, factor in heads:
-            scores = jnp.dot(qx[:, cols], keys_ref[...], preferred_element_type=F32)
+        products = [
+            jnp.dot(qx[:, cols], keys_ref[...], preferred_element_type=F32)
+            for cols, keys_ref, h, factor in heads
+        ]
+        for (cols, keys_ref, h, factor), scores in zip(heads, products):
             if first:
                 rows = lax.broadcasted_iota(jnp.int32, (384, 384), 0)
                 places = lax.broadcasted_iota(jnp.int32, (384, 384), 1)

time: 119 us -> 118 us (level)
  Pallas kernels: 118 us -> 116 us
    pallas_call x1, Pallas kernels: 118 us -> 116 us  [layer(): pl.pallas_call(functools.partial(layer_kernel, scale_one=scale_one, scale...]
where the time goes in v5:
time: 118 us; the launch traced here: 117 us
  Pallas kernels  116 us (98%)
  other arithmetic  1.58 us (1%)
    pallas_call x1, Pallas kernels, layer(): pl.pallas_call(functools.partial(layer_kernel, scale_one=scale_one, scale...  116 us

profile of v5, /device:TPU:2, one launch (start us, length us, event | category | flops | bytes accessed | tf_op | source)
XLA Modules:
  0.0 117.2 jit_solution(2120707155332525785)
XLA Ops:
  0.0 115.6 %layer.1 = f32[24,2048]{1,0:T(8,128)} custom-call(bf16[384,256]{1,0:T(8,128)(2,1)} %bitcast.16, bf16[64,384]{1,0:T(8,128)(2,1)} %bitcast.17, bf16[384,512]{1,0:T(8,128)(2,1)} %latent_ref.1, bf16[32,384]{1,0:T(8,128)(2,1)} %bitcast.18, f32[1,512]{1,0:T(1,128)} %bitcast.21, f32[16,1]{1,0:T(8,128)} %constant.2.clone.pace_ref, bf16[512,256]{1,0:T(8,128)(2,1)} %bitcast.14, ...), custom_call_target="tpu_custom_call" | custom-call | tf_op jit(solution)/shard_map/layer/pallas_call | solution.py:637
  115.6 1.6 %convert_element_type.3 = bf16[24,2048]{1,0:T(8,128)(2,1)} convert(f32[24,2048]{1,0:T(8,128)} %layer.1) | non-fusion elementwise | flops 49152 | bytes 294912 | tf_op jit(solution)/shard_map/convert_element_type | solution.py:743
